TPU v7x, 32 devices: a whole 2x2x4 slice. The times are simulated.
32 devices in a mesh: sp: 4 (over y, x), tp: 8 (over z, core).
Axes of the slice: x: 2, y: 2, z: 4, core: 2. Of those that a mesh axis runs over, the one named last changes fastest.
Arguments:
- cotangent: bfloat16 [1024, 2048], P('sp', 'tp'), may hold values from -6 to 6
- block_input: bfloat16 [1024, 2048], P('sp', 'tp'), may hold values from -6 to 6
- routes: int32 [1024, 2], P('sp'), may hold values from 0 to 3, all different within a row; in each aligned block of 256 rows (0 to 255, 256 to 511, ...) at most 160 rows name the same one
- route_weights: float32 [1024, 2], P('sp'), may hold values from 0.1 to 0.9
- gate_weight: bfloat16 [4, 2048, 7168], P('sp', None, 'tp'), may hold values from -0.125 to 0.125
- up_weight: bfloat16 [4, 2048, 7168], P('sp', None, 'tp'), may hold values from -0.125 to 0.125
- down_weight: bfloat16 [4, 7168, 2048], P('sp', 'tp'), may hold values from -0.0625 to 0.0625
- out_weight: bfloat16 [1024, 2048], P('tp'), may hold values from -0.1875 to 0.1875
- conv_out: bfloat16 [1024, 1024], P('tp', 'sp'), may hold values from -6 to 6
- gate_pre: bfloat16 [1024, 1024], P('tp', 'sp'), may hold values from -6 to 6
- prior_states: bfloat16 [1024, 1024], P('tp', 'sp'), may hold values from -6 to 6
- recur_weight: bfloat16 [16, 64, 64], replicated, may hold values from -0.75 to 0.75
- input_gate_matrix: bfloat16 [16, 64, 64], replicated, may hold values from -0.75 to 0.75
- decay_param: float32 [1024], replicated, may hold values from 4 to 16
- decay_jump: float32 [1024, 1024], P('tp', 'sp'), may hold values from -1 to 0, as said below
Outputs:
- gate_weight_grad: bfloat16 [4, 2048, 7168], P('sp', None, 'tp')
- up_weight_grad: bfloat16 [4, 2048, 7168], P('sp', None, 'tp')
- down_weight_grad: bfloat16 [4, 7168, 2048], P('sp', 'tp')
- out_weight_grad: float32 [1024, 2048], P('tp', 'sp')
- conv_grad: bfloat16 [1024, 1024], P('tp', 'sp')
- valve_logit_derivative: bfloat16 [1024, 1024], P('tp', 'sp')
Inputs may be any that keep to these rules, and one draw needn't show every extreme that they name: In each aligned block of 256 rows (the rows of one index of sp) no expert is named by more than 160 routes, a bound that some block reaches; a row names 2 different experts. `decay_jump`: every entry is at most -1 / 20480.
All inputs are finite; a program needn't handle non-finite values.
Results may differ from a plain program's by a relative error of at most 0.018.
Values may be sent and summed in bfloat16 or wider, within the bound.
A program may use at most 128 MiB of HBM per device.

v0:
```python
import functools

import jax
import jax.numpy as jnp
from jax import lax
from jax.experimental import pallas as pl
from jax.experimental.pallas import tpu as pltpu
from jax.sharding import PartitionSpec as P

HEAD_DIM = 64
TOP_K = 2


RATE_SCALE = 8.0


def link_pairs(left_pair, right_pair):
    return (left_pair[0] * right_pair[0], right_pair[0] * left_pair[1] + right_pair[1])


def routing_tables(routes, experts, capacity):
    flat_routes = routes.reshape(-1)
    onehot = (flat_routes[:, None] == jnp.arange(experts, dtype=jnp.int32)[None, :]).astype(
        jnp.int32
    )
    slot_rank = jnp.sum((jnp.cumsum(onehot, axis=0) - onehot) * onehot, axis=1)
    target = (flat_routes * capacity + slot_rank).reshape(routes.shape[0], routes.shape[1])
    slot_ids = jnp.arange(experts * capacity, dtype=jnp.int32)
    return jnp.transpose(target)[:, None, :] == slot_ids[None, :, None]


CORES = 2
VMEM = pl.BlockSpec(memory_space=pltpu.VMEM)


def across(place, step, size):
    result, bit = 0, 1
    while bit < size:
        result = result + lax.rem(lax.div(place, bit) + (step // bit) % 2, 2) * bit
        bit *= 2
    return result


def send(source, target, sems, index, device):
    return pltpu.make_async_remote_copy(
        src_ref=source,
        dst_ref=target,
        send_sem=sems[0].at[index],
        recv_sem=sems[1].at[index],
        device_id=device,
        device_id_type=pl.DeviceIdType.MESH,
    )


def greet(devices):
    barrier = pltpu.get_barrier_semaphore()
    for device in devices:
        pl.semaphore_signal(
            barrier, inc=1, device_id=device, device_id_type=pl.DeviceIdType.MESH
        )
    pl.semaphore_wait(barrier, len(devices))


def position(deep):
    sp, tp = lax.axis_index("sp"), lax.axis_index("tp")
    z, core = lax.div(tp, CORES), lax.rem(tp, CORES)
    return sp, tp, z, core, (sp, z * CORES + 1 - core)


def columns(block, width):
    return pl.ds(pl.multiple_of(block * width, width), width)


def dispatch_kernel(
    experts,
    deep,
    rows_in,
    cot_in,
    placing,
    slot_weight,
    rows_out,
    cot_out,
    held,
    stage,
    z_send,
    z_recv,
    p_send,
    p_recv,
    c_send,
    c_recv,
):
    sp, tp, z, core, partner = position(deep)
    width = rows_in.shape[1]
    planes = [(across(sp, k, experts), tp) for k in range(experts)]
    levels = [across(z, d, deep) for d in range(deep)]
    lines = [(sp, level * CORES + core) for level in levels]
    greet(planes[1:] + lines[1:] + [partner])
    sources, outs = (rows_in, cot_in), (rows_out, cot_out)
    line_copies, plane_copies = {}, {}
    for a in range(2):
        for d in range(1, deep):
            copy = send(sources[a], held.at[a, d - 1], (z_send, z_recv), (a, d), lines[d])
            copy.start()
            line_copies[a, d] = copy
    own_first = [(0, 0), (1, 0)] + [(a, d) for a in range(2) for d in range(1, deep)]
    for a, d in own_first:
            if d:
                line_copies[a, d].wait_recv()
            block = held[a, d - 1] if d else sources[a][...]
            here = columns(levels[d] * CORES + core, width)
            for k in list(range(1, experts)) + [0]:
                expert = planes[k][0]
                piece = jnp.dot(placing[expert], block, preferred_element_type=jnp.float32)
                if a:
                    piece = piece * slot_weight[expert]
                piece = piece.astype(jnp.bfloat16)
                if k == 0:
                    outs[a][sp, :, here] = piece
                else:
                    stage[a, d, k - 1] = piece
                    copy = send(
                        stage.at[a, d, k - 1],
                        outs[a].at[sp, :, here],
                        (p_send, p_recv),
                        (a, d, k),
                        planes[k],
                    )
                    copy.start()
                    plane_copies[a, d, k] = copy
    core_copies = []
    for a in range(2):
        for d in range(deep):
            for k in range(1, experts):
                plane_copies[a, d, k].wait_recv()
            here = columns(levels[d] * CORES + core, width)
            copy = send(
                outs[a].at[:, :, here], outs[a].at[:, :, here], (c_send, c_recv), (a, d), partner
            )
            copy.start()
            core_copies.append(copy)
    for copy in core_copies:
        copy.wait_recv()
    for copy in core_copies + list(plane_copies.values()) + list(line_copies.values()):
        copy.wait_send()


def dispatch(rows_in, cot_in, placing, slot_weight):
    experts, capacity, tok_rows = placing.shape
    deep = lax.axis_size("tp") // CORES
    width = rows_in.shape[1]
    out = jax.ShapeDtypeStruct((experts, capacity, width * deep * CORES), jnp.bfloat16)
    sems = [(2, deep), (2, deep, experts), (2, deep)]
    return pl.pallas_call(
        functools.partial(dispatch_kernel, experts, deep),
        out_shape=(out, out),
        in_specs=[VMEM] * 4,
        out_specs=(VMEM, VMEM),
        scratch_shapes=[
            pltpu.VMEM((2, deep - 1, tok_rows, width), jnp.bfloat16),
            pltpu.VMEM((2, deep, experts - 1, capacity, width), jnp.bfloat16),
        ]
        + [pltpu.SemaphoreType.DMA(shape) for shape in sems for _ in range(2)],
        compiler_params=pltpu.CompilerParams(
            collective_id=0, has_side_effects=True, vmem_limit_bytes=48 << 20
        ),
    )(rows_in, cot_in, placing, slot_weight)


def combine_kernel(
    experts,
    deep,
    parts,
    cot_in,
    taking,
    full_out,
    paired,
    stage,
    plane,
    line_out,
    line_in,
    c_send,
    c_recv,
    p_send,
    p_recv,
    z_send,
    z_recv,
    g_send,
    g_recv,
    f_send,
    f_recv,
):
    sp, tp, z, core, partner = position(deep)
    width = cot_in.shape[1]
    planes = [(across(sp, k, experts), tp) for k in range(experts)]
    levels = [across(z, d, deep) for d in range(deep)]
    lines = [(sp, level * CORES + core) for level in levels]
    greet(planes[1:] + lines[1:] + [partner])
    order = list(range(deep - 1, -1, -1))
    started, core_copies, plane_copies, line_copies = [], {}, {}, {}
    for d in order:
        theirs = columns(levels[d] * CORES + 1 - core, width)
        copy = send(parts.at[:, :, theirs], paired.at[d], (c_send, c_recv), d, partner)
        copy.start()
        core_copies[d] = copy
        started.append(copy)
    for d in order:
        core_copies[d].wait_recv()
        here = columns(levels[d] * CORES + core, width)
        for k in list(range(1, experts)) + [0]:
            home = planes[k][0]
            piece = (
                parts[home, :, here].astype(jnp.float32) + paired[d, home].astype(jnp.float32)
            ).astype(jnp.bfloat16)
            if k == 0:
                plane[d, 0] = piece
            else:
                stage[d, k - 1] = piece
                copy = send(
                    stage.at[d, k - 1], plane.at[d, k], (p_send, p_recv), (d, k), planes[k]
                )
                copy.start()
                plane_copies[d, k] = copy
                started.append(copy)
    total = cot_in[...].astype(jnp.float32)
    for d in order:
        summed = jnp.dot(taking[sp], plane[d, 0], preferred_element_type=jnp.float32)
        for k in range(1, experts):
            plane_copies[d, k].wait_recv()
            summed = summed + jnp.dot(
                taking[planes[k][0]], plane[d, k], preferred_element_type=jnp.float32
            )
        if d == 0:
            total = total + summed
        else:
            line_out[d - 1] = summed.astype(jnp.bfloat16)
            copy = send(line_out.at[d - 1], line_in.at[d - 1], (z_send, z_recv), d, lines[d])
            copy.start()
            line_copies[d] = copy
            started.append(copy)
    for d in order[:-1]:
        line_copies[d].wait_recv()
        total = total + line_in[d - 1].astype(jnp.float32)
    mine = columns(tp, width)
    full_out[:, mine] = total.astype(jnp.bfloat16)
    gathers, forwards = {}, []
    for d in range(1, deep):
        copy = send(full_out.at[:, mine], full_out.at[:, mine], (g_send, g_recv), d, lines[d])
        copy.start()
        gathers[d] = copy
        started.append(copy)
    for d in range(deep):
        if d:
            gathers[d].wait_recv()
        here = columns(levels[d] * CORES + core, width)
        copy = send(full_out.at[:, here], full_out.at[:, here], (f_send, f_recv), d, partner)
        copy.start()
        forwards.append(copy)
    for copy in forwards:
        copy.wait_recv()
    for copy in started + forwards:
        copy.wait_send()


def combine(parts, cot_in, taking):
    experts, capacity, full_width = parts.shape
    tok_rows, width = cot_in.shape
    deep = lax.axis_size("tp") // CORES
    sems = [(deep,), (deep, experts), (deep,), (deep,), (deep,)]
    return pl.pallas_call(
        functools.partial(combine_kernel, experts, deep),
        out_shape=jax.ShapeDtypeStruct((tok_rows, full_width), jnp.bfloat16),
        in_specs=[VMEM] * 3,
        out_specs=VMEM,
        scratch_shapes=[
            pltpu.VMEM((deep, experts, capacity, width), jnp.bfloat16),
            pltpu.VMEM((deep, experts - 1, capacity, width), jnp.bfloat16),
            pltpu.VMEM((deep, experts, capacity, width), jnp.bfloat16),
            pltpu.VMEM((deep - 1, tok_rows, width), jnp.bfloat16),
            pltpu.VMEM((deep - 1, tok_rows, width), jnp.bfloat16),
        ]
        + [pltpu.SemaphoreType.DMA(shape) for shape in sems for _ in range(2)],
        compiler_params=pltpu.CompilerParams(
            collective_id=1, has_side_effects=True, vmem_limit_bytes=48 << 20
        ),
    )(parts, cot_in, taking)


def closing_kernel(
    count, summary, product, summaries, products, s_send, s_recv, p_send, p_recv
):
    sp, tp = lax.axis_index("sp"), lax.axis_index("tp")
    width = products.shape[2]
    peers = [(across(sp, k, count), tp) for k in range(count)]
    greet(peers[1:])
    copies = []
    for k in range(1, count):
        copies.append(send(summary, summaries.at[sp], (s_send, s_recv), k, peers[k]))
        copies[-1].start()
    for k in range(1, count):
        theirs = columns(peers[k][0], width)
        copies.append(
            send(product.at[:, theirs], products.at[k], (p_send, p_recv), k, peers[k])
        )
        copies[-1].start()
    summaries[sp] = summary[...]
    products[0] = product[:, columns(sp, width)]
    for copy in copies:
        copy.wait()


def closing(summary, product):
    count = lax.axis_size("sp")
    channels, full_width = product.shape
    return pl.pallas_call(
        functools.partial(closing_kernel, count),
        out_shape=(
            jax.ShapeDtypeStruct((count,) + summary.shape, summary.dtype),
            jax.ShapeDtypeStruct((count, channels, full_width // count), product.dtype),
        ),
        in_specs=[VMEM] * 2,
        out_specs=(VMEM, VMEM),
        scratch_shapes=[pltpu.SemaphoreType.DMA((count,)) for _ in range(4)],
        compiler_params=pltpu.CompilerParams(
            collective_id=2, has_side_effects=True, vmem_limit_bytes=16 << 20
        ),
    )(summary, product)


def expert_work(slot_rows, slot_cot, w_gate, w_up, w_down):
    minor = (((1,), (1,)), ((), ()))
    gate_act = jnp.dot(slot_rows, w_gate, preferred_element_type=jnp.float32)
    up_act = jnp.dot(slot_rows, w_up, preferred_element_type=jnp.float32)
    sigma_gate = jax.nn.sigmoid(gate_act)
    silu_val = gate_act * sigma_gate
    hidden = (silu_val * up_act).astype(jnp.bfloat16)
    d_hidden = lax.dot_general(slot_cot, w_down, minor, preferred_element_type=jnp.float32)
    d_gate = (d_hidden * up_act * sigma_gate * (1.0 + gate_act * (1.0 - sigma_gate))).astype(
        jnp.bfloat16
    )
    d_up = (d_hidden * silu_val).astype(jnp.bfloat16)
    width_part = lax.dot_general(d_gate, w_gate, minor, preferred_element_type=jnp.float32)
    width_part = width_part + lax.dot_general(d_up, w_up, minor, preferred_element_type=jnp.float32)
    return (hidden, d_gate, d_up, width_part)


def weight_grads(slot_rows, slot_cot, hidden, d_gate, d_up):
    major = (((0,), (0,)), ((), ()))
    gate_grad = lax.dot_general(
        slot_rows, d_gate, major, preferred_element_type=jnp.float32
    ).astype(jnp.bfloat16)
    up_grad = lax.dot_general(slot_rows, d_up, major, preferred_element_type=jnp.float32).astype(
        jnp.bfloat16
    )
    down_grad = lax.dot_general(hidden, slot_cot, major, preferred_element_type=jnp.float32).astype(
        jnp.bfloat16
    )
    return (gate_grad[None], up_grad[None], down_grad[None])


def local(
    cotangent,
    block_input,
    routes,
    route_weights,
    gate_weight,
    up_weight,
    down_weight,
    out_weight,
    conv_out,
    gate_pre,
    prior_states,
    recur_weight,
    input_gate_matrix,
    decay_param,
    decay_jump,
):
    experts = lax.axis_size("sp")
    tok_rows = cotangent.shape[0]
    capacity = 5 * tok_rows * TOP_K // (4 * experts)
    route_hits = routing_tables(routes, experts, capacity)
    hits = jnp.sum(route_hits.astype(jnp.float32), axis=0)
    placing = hits.astype(jnp.bfloat16).reshape(experts, capacity, tok_rows)
    taking = jnp.swapaxes(placing, 1, 2)
    slot_weight = jnp.sum(
        jnp.where(route_hits, jnp.transpose(route_weights)[:, None, :], 0.0), axis=(0, 2)
    ).reshape(experts, capacity, 1)
    got_rows, got_cot = dispatch(block_input, cotangent, placing, slot_weight)
    full_width = got_rows.shape[2]
    slot_rows = got_rows.reshape(-1, full_width)
    slot_cot = got_cot.reshape(-1, full_width)
    hidden, d_gate, d_up, width_part = expert_work(
        slot_rows, slot_cot, gate_weight[0], up_weight[0], down_weight[0]
    )
    gate_grad, up_grad, down_grad = weight_grads(slot_rows, slot_cot, hidden, d_gate, d_up)
    full_grad = combine(
        width_part.astype(jnp.bfloat16).reshape(experts, capacity, full_width), cotangent, taking
    )
    channels = conv_out.shape[0]
    length = conv_out.shape[1]
    head_count = channels // HEAD_DIM
    head_start = lax.axis_index("tp") * head_count
    w_recur = lax.dynamic_slice_in_dim(recur_weight, head_start, head_count, 0)
    w_input = lax.dynamic_slice_in_dim(input_gate_matrix, head_start, head_count, 0)
    rate_parameter = lax.dynamic_slice_in_dim(decay_param, head_start * HEAD_DIM, channels, 0)[
        :, None
    ]
    shaped = conv_out.reshape(head_count, HEAD_DIM, length)
    recur_gate = jax.nn.sigmoid(
        jnp.einsum("hij,hit->hjt", w_recur, shaped, preferred_element_type=jnp.float32).reshape(
            channels, length
        )
    )
    input_gate = jax.nn.sigmoid(
        jnp.einsum("hij,hit->hjt", w_input, shaped, preferred_element_type=jnp.float32).reshape(
            channels, length
        )
    )
    softened = jax.nn.softplus(-rate_parameter)
    log_decay = -RATE_SCALE * recur_gate * softened + decay_jump
    decay_val = jnp.exp(log_decay)
    norm_scale = jnp.sqrt(-jnp.expm1(2.0 * log_decay))
    conv_vals = conv_out.astype(jnp.float32)
    prior_vals = prior_states.astype(jnp.float32)
    state = decay_val * prior_vals + norm_scale * input_gate * conv_vals
    gelu_val, gelu_pull = jax.vjp(jax.nn.gelu, gate_pre.astype(jnp.float32))
    mixed = (gelu_val * state).astype(jnp.bfloat16)
    d_mixed = lax.dot_general(
        out_weight, full_grad, (((1,), (1,)), ((), ())), preferred_element_type=jnp.float32
    )
    valve_logit_derivative = gelu_pull(d_mixed * state)[0].astype(jnp.bfloat16)
    d_state = d_mixed * gelu_val
    shifted = jnp.concatenate([decay_val[:, 1:], jnp.ones((channels, 1), jnp.float32)], axis=1)
    flipped = lax.associative_scan(link_pairs, (jnp.flip(shifted, 1), jnp.flip(d_state, 1)), axis=1)
    decay_prod = jnp.flip(flipped[0], 1)
    local_sum = jnp.flip(flipped[1], 1)
    summary = jnp.stack([decay_val[:, 0] * decay_prod[:, 0], decay_val[:, 0] * local_sum[:, 0]])
    product = jnp.dot(mixed, full_grad, preferred_element_type=jnp.float32).astype(jnp.bfloat16)
    summaries, products = closing(summary, product)
    carried = jnp.zeros((channels,), jnp.float32)
    for later in range(experts - 1, 0, -1):
        longer = summaries[later, 1] + summaries[later, 0] * carried
        carried = jnp.where(later > lax.axis_index("sp"), longer, carried)
    out_weight_grad = jnp.sum(products.astype(jnp.float32), axis=0)
    state_grad = local_sum + decay_prod * carried[:, None]
    grad_log = (
        state_grad * prior_vals * decay_val
        - state_grad * input_gate * conv_vals * decay_val * decay_val / norm_scale
    )
    grad_recur = (grad_log * -RATE_SCALE * softened * recur_gate * (1.0 - recur_gate)).astype(
        jnp.bfloat16
    )
    grad_input = (state_grad * norm_scale * conv_vals * input_gate * (1.0 - input_gate)).astype(
        jnp.bfloat16
    )
    back_recur = jnp.einsum(
        "hij,hjt->hit",
        w_recur,
        grad_recur.reshape(head_count, HEAD_DIM, length),
        preferred_element_type=jnp.float32,
    ).reshape(channels, length)
    back_input = jnp.einsum(
        "hij,hjt->hit",
        w_input,
        grad_input.reshape(head_count, HEAD_DIM, length),
        preferred_element_type=jnp.float32,
    ).reshape(channels, length)
    conv_grad = (state_grad * norm_scale * input_gate + back_recur + back_input).astype(
        jnp.bfloat16
    )
    return (gate_grad, up_grad, down_grad, out_weight_grad, conv_grad, valve_logit_derivative)


def solution(mesh):
    in_specs = (
        P("sp", "tp"),
        P("sp", "tp"),
        P("sp", None),
        P("sp", None),
        P("sp", None, "tp"),
        P("sp", None, "tp"),
        P("sp", "tp", None),
        P("tp", None),
        P("tp", "sp"),
        P("tp", "sp"),
        P("tp", "sp"),
        P(),
        P(),
        P(),
        P("tp", "sp"),
    )
    out_specs = (
        P("sp", None, "tp"),
        P("sp", None, "tp"),
        P("sp", "tp", None),
        P("tp", "sp"),
        P("tp", "sp"),
        P("tp", "sp"),
    )
    return jax.shard_map(local, mesh=mesh, in_specs=in_specs, out_specs=out_specs, check_vma=False)
```

profile of v0, /device:TPU:0, one launch (start us, length us, event | category | flops | bytes accessed | tf_op | source)
XLA Modules:
  0.0 145.6 jit_solution(12163601371138688153)
XLA Ops:
  0.6 0.0 copy-start
  0.6 0.9 copy.102
  1.5 0.1 eq.42
  1.7 1.2 reduce-window.6
  2.9 0.2 slice_reduce_fusion
  3.1 0.2 reduce-window.9
  3.3 0.1 add_bitcast_fusion
  3.4 0.1 eq.38
  3.6 0.1 reduce_sum.39
  3.7 0.1 copy.104
  3.8 0.7 add_bitcast_fusion.1
  4.5 1.0 select_reduce_fusion
  5.5 0.2 reshape.173.slot_weight
  5.7 0.0 copy-start.2
  5.7 0.9 copy-done.2
  6.6 0.9 copy-done.4
  7.5 38.4 %shard_map.190 = (bf16[4,160,2048]{2,1,0:T(8,128)(2,1)S(1)}, bf16[4,160,2048]{2,1,0:T(8,128)(2,1)S(1)}) custom-call(bf16[256,256]{1,0:T(8,128)(2,1)S(1)} %copy-done.4, bf16[256,256]{1,0:T(8,128)(2,1)S(1)} %copy-done.2, bf16[4,160,256]{2,1,0:T(8,128)(2,1)S(1)} %bitcast.106, f32[4,160,1]{2,1,0:T(8,128)S(1)} %reshape.173.slot_weight), custom_call_target="tpu_custom_call" | custom-call | tf_op jit(solution)/shard_map/pallas_call | solution.py:153
  46.0 0.0 copy-start.7
  46.0 0.0 copy-start.5
  46.0 0.0 copy-start.15
  46.0 6.8 %fusion.2 = f32[640,896]{1,0:T(8,128)S(1)} fusion(bf16[640,2048]{1,0:T(8,128)(2,1)S(1)} %bitcast.112, bf16[1,2048,896]{2,1,0:T(8,128)(2,1)} %param.19), kind=kOutput, calls=%fused_computation.3 | convolution fusion | flops 2348810240 | bytes 8585216 | tf_op jit(solution)/shard_map/dot_general | solution.py:331
  52.9 0.0 copy-start.13
  52.9 2.9 %fusion.6 = f32[640,896]{1,0:T(8,128)S(1)} fusion(bf16[640,2048]{1,0:T(8,128)(2,1)S(1)} %bitcast.113, bf16[1,2048,896]{2,1,0:T(8,128)(2,1)S(1)} %copy-done.15), kind=kOutput, calls=%fused_computation.7 | convolution fusion | flops 2348810240 | bytes 8585216 | tf_op jit(solution)/shard_map/dot_general | solution.py:332
  55.8 0.0 copy-start.20
  55.8 0.0 copy-done.5
  55.8 0.0 copy-done.18
  55.8 0.0 copy-done.13
  55.8 0.0 copy-start.14
  55.8 3.6 %multiply_convert_fusion.1 = (bf16[640,896]{1,0:T(8,128)(2,1)S(1)}, bf16[640,896]{1,0:T(8,128)(2,1)S(1)}) fusion(f32[640,896]{1,0:T(8,128)S(1)} %fusion.2, f32[640,896]{1,0:T(8,128)S(1)} %fusion.6, bf16[640,2048]{1,0:T(8,128)(2,1)S(1)} %bitcast.110, bf16[1,896,2048]{2,1,0:T(8,128)(2,1)S(1)} %copy-done.13), kind=kOutput, calls=%fused_computation.16 | convolution fusion | flops 2356264960 | bytes 13172736 | tf_op jit(solution)/shard_map/dot_general | solution.py:336
  59.4 0.0 copy-start.16
  59.4 2.9 %fusion = f32[640,2048]{1,0:T(8,128)S(1)} fusion(bf16[640,896]{1,0:T(8,128)(2,1)S(1)} %get-tuple-element.45, bf16[1,2048,896]{2,1,0:T(8,128)(2,1)S(1)} %copy-done.14), kind=kOutput, calls=%fused_computation.1 | convolution fusion | flops 2348810240 | bytes 10059776 | tf_op jit(solution)/shard_map/dot_general | solution.py:341
  62.4 0.0 copy-start.3
  62.4 4.4 %add_convert_fusion = bf16[640,2048]{1,0:T(8,128)(2,1)} fusion(f32[640,2048]{1,0:T(8,128)S(1)} %fusion, bf16[640,896]{1,0:T(8,128)(2,1)S(1)} %get-tuple-element.44, bf16[1,2048,896]{2,1,0:T(8,128)(2,1)S(1)} %copy-done.15), kind=kOutput, calls=%fused_computation | convolution fusion | flops 2351431680 | bytes 12681216 | tf_op jit(solution)/shard_map/dot_general | solution.py:342
  66.8 0.2 copy.109
  67.0 0.0 copy-start.1
  67.0 1.7 %copy-done.1 = bf16[640,2048]{1,0:T(8,128)(2,1)S(1)} copy-done((bf16[640,2048]{1,0:T(8,128)(2,1)S(1)}, bf16[640,2048]{1,0:T(8,128)(2,1)}, u32[]{:S(2)}) %copy-start.1) | copy-done | bytes 2621464
  68.8 38.5 %shard_map.191 = bf16[256,2048]{1,0:T(8,128)(2,1)S(1)} custom-call(bf16[4,160,2048]{2,1,0:T(8,128)(2,1)S(1)} %bitcast.108, bf16[256,256]{1,0:T(8,128)(2,1)S(1)} %copy-done.3, bf16[4,256,160]{2,1,0:T(8,128)(2,1)S(1)} %bitcast.109), custom_call_target="tpu_custom_call" | custom-call | tf_op jit(solution)/shard_map/pallas_call | solution.py:269
  107.3 1.0 fusion.18
  108.3 0.1 copy.113
  108.4 1.0 fusion.16
  109.4 0.1 copy.107
  109.5 0.8 fusion.61
  110.2 0.1 copy.111
  110.4 0.1 copy.114
  110.5 0.1 copy.110
  110.6 0.1 copy.108
  110.7 0.5 fusion.30
  113.3 0.1 rev.10
  113.5 0.1 rev.9
  113.6 0.5 convolution_convert_fusion.product
  114.1 9.8 %shard_map.192 = (f32[4,2,128]{2,1,0:T(2,128)S(1)}, bf16[4,128,512]{2,1,0:T(8,128)(2,1)S(1)}) custom-call(f32[2,128]{1,0:T(2,128)S(1)} %pad_maximum_fusion.13.summary, bf16[128,2048]{1,0:T(8,128)(2,1)S(1)} %convolution_convert_fusion.product), custom_call_target="tpu_custom_call" | custom-call | tf_op jit(solution)/shard_map/pallas_call | solution.py:314
  123.9 0.2 fusion.33
  124.1 0.1 copy.119
  124.2 0.9 fusion.52
  125.1 0.1 copy.121
  125.2 0.1 copy.124
  125.4 0.9 fusion.49
  126.3 0.1 copy.126
  126.4 0.7 copy.127
  127.1 0.8 convert_reduce_fusion.1
  127.9 0.7 copy.128
  128.7 7.4 %convert_bitcast_fusion.1 = bf16[1,2048,896]{2,1,0:T(8,128)(2,1)} fusion(bf16[640,2048]{1,0:T(8,128)(2,1)} %bitcast.114, bf16[640,896]{1,0:T(8,128)(2,1)} %copy-done.22), kind=kOutput, calls=%fused_computation.12 | convolution fusion | flops 2350645248 | bytes 7438336 | tf_op jit(solution)/shard_map/dot_general | solution.py:351
  136.1 4.9 %convert_bitcast_fusion.2 = bf16[1,2048,896]{2,1,0:T(8,128)(2,1)} fusion(bf16[640,2048]{1,0:T(8,128)(2,1)S(1)} %bitcast.115, bf16[640,896]{1,0:T(8,128)(2,1)S(1)} %copy-done.17), kind=kOutput, calls=%fused_computation.13 | convolution fusion | flops 2350645248 | bytes 7438336 | tf_op jit(solution)/shard_map/dot_general | solution.py:348
  140.9 4.6 %convert_bitcast_fusion = bf16[1,896,2048]{2,1,0:T(8,128)(2,1)} fusion(bf16[640,2048]{1,0:T(8,128)(2,1)S(1)} %bitcast.111, f32[640,896]{1,0:T(8,128)S(1)} %copy-done.21, f32[640,896]{1,0:T(8,128)S(1)} %copy-done.19), kind=kOutput, calls=%fused_computation.11 | convolution fusion | flops 2354085888 | bytes 10878976 | tf_op jit(solution)/shard_map/dot_general | solution.py:354
  (167 shorter events, 1.6 us)
Async XLA Ops:
  0.6 110.1 %copy-start = (bf16[128,2048]{1,0:T(8,128)(2,1)S(1)}, bf16[128,2048]{1,0:T(8,128)(2,1)}, u32[]{:S(2)}) copy-start(bf16[128,2048]{1,0:T(8,128)(2,1)} %param.22) | copy-start | bytes 1572868
  5.7 0.9 copy-start.2
  6.6 0.9 copy-start.4
  46.0 6.9 %copy-start.7 = (bf16[4,160,2048]{2,1,0:T(8,128)(2,1)}, bf16[4,160,2048]{2,1,0:T(8,128)(2,1)S(1)}, u32[]{:S(2)}) copy-start(bf16[4,160,2048]{2,1,0:T(8,128)(2,1)S(1)} %get-tuple-element.10) | copy-start | bytes 7864324
  46.0 9.8 %copy-start.5 = (bf16[4,160,2048]{2,1,0:T(8,128)(2,1)}, bf16[4,160,2048]{2,1,0:T(8,128)(2,1)S(1)}, u32[]{:S(2)}) copy-start(bf16[4,160,2048]{2,1,0:T(8,128)(2,1)S(1)} %get-tuple-element.11) | copy-start | bytes 7864324
  46.0 6.9 %copy-start.15 = (bf16[1,2048,896]{2,1,0:T(8,128)(2,1)S(1)}, bf16[1,2048,896]{2,1,0:T(8,128)(2,1)}, u32[]{:S(2)}) copy-start(bf16[1,2048,896]{2,1,0:T(8,128)(2,1)} %param.20) | copy-start | bytes 11010052
  52.9 2.9 %copy-start.18 = (f32[640,896]{1,0:T(8,128)}, f32[640,896]{1,0:T(8,128)S(1)}, u32[]{:S(2)}) copy-start(f32[640,896]{1,0:T(8,128)S(1)} %fusion.2) | copy-start | bytes 6881284
  52.9 2.9 %copy-start.13 = (bf16[1,896,2048]{2,1,0:T(8,128)(2,1)S(1)}, bf16[1,896,2048]{2,1,0:T(8,128)(2,1)}, u32[]{:S(2)}) copy-start(bf16[1,896,2048]{2,1,0:T(8,128)(2,1)} %param.21) | copy-start | bytes 11010052
  55.8 3.6 %copy-start.20 = (f32[640,896]{1,0:T(8,128)}, f32[640,896]{1,0:T(8,128)S(1)}, u32[]{:S(2)}) copy-start(f32[640,896]{1,0:T(8,128)S(1)} %fusion.6) | copy-start | bytes 6881284
  55.8 3.6 %copy-start.14 = (bf16[1,2048,896]{2,1,0:T(8,128)(2,1)S(1)}, bf16[1,2048,896]{2,1,0:T(8,128)(2,1)}, u32[]{:S(2)}) copy-start(bf16[1,2048,896]{2,1,0:T(8,128)(2,1)} %param.19) | copy-start | bytes 11010052
  59.4 3.0 %copy-start.16 = (bf16[640,896]{1,0:T(8,128)(2,1)}, bf16[640,896]{1,0:T(8,128)(2,1)S(1)}, u32[]{:S(2)}) copy-start(bf16[640,896]{1,0:T(8,128)(2,1)S(1)} %get-tuple-element.45) | copy-start | bytes 3440644
  59.4 2.9 %copy-start.22 = (bf16[640,896]{1,0:T(8,128)(2,1)}, bf16[640,896]{1,0:T(8,128)(2,1)S(1)}, u32[]{:S(2)}) copy-start(bf16[640,896]{1,0:T(8,128)(2,1)S(1)} %get-tuple-element.44) | copy-start | bytes 3440644
  62.4 4.6 %copy-start.3 = (bf16[256,256]{1,0:T(8,128)(2,1)S(1)}, bf16[256,256]{1,0:T(8,128)(2,1)}, u32[]{:S(2)}) copy-start(bf16[256,256]{1,0:T(8,128)(2,1)} %cot_in.3) | copy-start | bytes 393220
  67.0 1.7 %copy-start.1 = (bf16[640,2048]{1,0:T(8,128)(2,1)S(1)}, bf16[640,2048]{1,0:T(8,128)(2,1)}, u32[]{:S(2)}) copy-start(bf16[640,2048]{1,0:T(8,128)(2,1)} %add_convert_fusion) | copy-start | bytes 7864324
  68.7 38.5 %copy-start.11 = (bf16[128,256]{1,0:T(8,128)(2,1)S(1)}, bf16[128,256]{1,0:T(8,128)(2,1)}, u32[]{:S(2)}) copy-start(bf16[128,256]{1,0:T(8,128)(2,1)} %param.23) | copy-start | bytes 196612
  68.7 41.5 %copy-start.10 = (bf16[128,256]{1,0:T(8,128)(2,1)S(1)}, bf16[128,256]{1,0:T(8,128)(2,1)}, u32[]{:S(2)}) copy-start(bf16[128,256]{1,0:T(8,128)(2,1)} %param.25) | copy-start | bytes 196612
  68.7 41.8 %copy-start.12 = (bf16[128,256]{1,0:T(8,128)(2,1)S(1)}, bf16[128,256]{1,0:T(8,128)(2,1)}, u32[]{:S(2)}) copy-start(bf16[128,256]{1,0:T(8,128)(2,1)} %param.24) | copy-start | bytes 196612
  68.7 41.9 %copy-start.9 = (f32[128,256]{1,0:T(8,128)S(1)}, f32[128,256]{1,0:T(8,128)}, u32[]{:S(2)}) copy-start(f32[128,256]{1,0:T(8,128)} %param.29) | copy-start | bytes 393220
  128.7 7.4 %copy-start.8 = (bf16[4,160,2048]{2,1,0:T(8,128)(2,1)S(1)}, bf16[4,160,2048]{2,1,0:T(8,128)(2,1)}, u32[]{:S(2)}) copy-start(bf16[4,160,2048]{2,1,0:T(8,128)(2,1)} %copy-done.7) | copy-start | bytes 7864324
  128.7 7.4 %copy-start.17 = (bf16[640,896]{1,0:T(8,128)(2,1)S(1)}, bf16[640,896]{1,0:T(8,128)(2,1)}, u32[]{:S(2)}) copy-start(bf16[640,896]{1,0:T(8,128)(2,1)} %copy-done.16) | copy-start | bytes 3440644
  136.1 4.9 %copy-start.6 = (bf16[4,160,2048]{2,1,0:T(8,128)(2,1)S(1)}, bf16[4,160,2048]{2,1,0:T(8,128)(2,1)}, u32[]{:S(2)}) copy-start(bf16[4,160,2048]{2,1,0:T(8,128)(2,1)} %copy-done.5) | copy-start | bytes 7864324
  136.1 4.9 %copy-start.19 = (f32[640,896]{1,0:T(8,128)S(1)}, f32[640,896]{1,0:T(8,128)}, u32[]{:S(2)}) copy-start(f32[640,896]{1,0:T(8,128)} %copy-done.18) | copy-start | bytes 6881284
  136.1 4.9 %copy-start.21 = (f32[640,896]{1,0:T(8,128)S(1)}, f32[640,896]{1,0:T(8,128)}, u32[]{:S(2)}) copy-start(f32[640,896]{1,0:T(8,128)} %copy-done.20) | copy-start | bytes 6881284
where the time goes:
time: 146 us
  Pallas kernels  86.7 us (59%)
  matrix products  42.2 us (29%)
  local copies, waits for them, and re-layouts  9.39 us (6%)
  other arithmetic  5.45 us (4%)
  between operations  1.83 us (1%)
    pallas_call x1, Pallas kernels, combine(): pl.pallas_call(functools.partial(combine_kernel, experts, deep), out_shap...  38.5 us
    pallas_call x1, Pallas kernels, dispatch(): pl.pallas_call(functools.partial(dispatch_kernel, experts, deep), out_sha...  38.4 us
    pallas_call x1, Pallas kernels, closing(): pl.pallas_call(functools.partial(closing_kernel, count), out_shape=(jax.S...  9.76 us
    dot_general x1, matrix products, weight_grads(): lax.dot_general(slot_rows, d_up, major, preferred_element_type=jnp.float32)  7.39 us
    dot_general x1, matrix products, expert_work(): gate_act = jnp.dot(slot_rows, w_gate, preferred_element_type=jnp.float32)  6.84 us
    unnamed x53, local copies, waits for them, and re-layouts  6.42 us
    dot_general x1, matrix products, weight_grads(): lax.dot_general(slot_rows, d_gate, major, preferred_element_type=jnp.floa...  4.85 us
    dot_general x1, matrix products, weight_grads(): lax.dot_general(hidden, slot_cot, major, preferred_element_type=jnp.float32)  4.6 us

commit v1 on v0

v1 whole, which is shorter than its diff:
```python
import functools

import jax
import jax.numpy as jnp
from jax import lax
from jax.experimental import pallas as pl
from jax.experimental.pallas import tpu as pltpu
from jax.sharding import PartitionSpec as P

HEAD_DIM = 64
TOP_K = 2
RATE_SCALE = 8.0
CORES = 2
NN = (((1,), (0,)), ((), ()))
NT = (((1,), (1,)), ((), ()))
TN = (((0,), (0,)), ((), ()))
F32 = jnp.float32
BF16 = jnp.bfloat16


def dot(a, b, dims=NN):
    return lax.dot_general(a, b, dims, preferred_element_type=F32)


def across(place, step, size):
    result, bit = 0, 1
    while bit < size:
        result = result + lax.rem(lax.div(place, bit) + (step // bit) % 2, 2) * bit
        bit *= 2
    return result


def span(block, width):
    return pl.ds(pl.multiple_of(block * width, width), width)


def greet(devices):
    barrier = pltpu.get_barrier_semaphore()
    for device in devices:
        pl.semaphore_signal(
            barrier, inc=1, device_id=device, device_id_type=pl.DeviceIdType.MESH
        )
    pl.semaphore_wait(barrier, len(devices))


def log1p_small(y):
    series = y * (1.0 + y * (-0.5 + y * (1.0 / 3 + y * (-0.25 + y * (0.2 - y / 6.0)))))
    return jnp.where(y < 0.03125, series, jnp.log(1.0 + y))


def expm1_neg(x):
    series = 1.0 / 40320 * x + 1.0 / 5040
    for factor in (720, 120, 24, 6, 2):
        series = series * x + 1.0 / factor
    series = x * (series * x + 1.0)
    return jnp.where(x > -0.35, series, jnp.exp(x) - 1.0)


class Copies:
    def __init__(self, send_sems, recv_sems):
        self.sems = (send_sems, recv_sems)
        self.count = 0
        self.sent = []

    def start(self, source, target, device):
        copy = pltpu.make_async_remote_copy(
            src_ref=source,
            dst_ref=target,
            send_sem=self.sems[0].at[self.count],
            recv_sem=self.sems[1].at[self.count],
            device_id=device,
            device_id_type=pl.DeviceIdType.MESH,
        )
        copy.start()
        self.count += 1
        self.sent.append(copy)
        return copy


INPUTS = (
    "rows_hbm", "cot_hbm", "routes", "route_w", "wg_hbm", "wu_hbm", "wd_hbm", "ow_hbm",
    "conv_hbm", "pre_hbm", "prior_hbm", "wr_hbm", "wi_hbm", "rate", "jump_hbm",
)
OUTPUTS = ("gate_grad", "up_grad", "down_grad", "out_grad", "conv_grad", "valve")


class Refs:
    pass


def kernel(names, experts, deep, cap, *refs):
    r = Refs()
    for name, ref in zip(names, refs):
        setattr(r, name, ref)
    sp, tp = lax.axis_index("sp"), lax.axis_index("tp")
    z, core = lax.div(tp, CORES), lax.rem(tp, CORES)
    partner = (sp, z * CORES + 1 - core)
    planes = [(across(sp, k, experts), tp) for k in range(experts)]
    levels = [across(z, d, deep) for d in range(deep)]
    lines = [(sp, level * CORES + core) for level in levels]
    tokens, width = r.rows.shape
    pair = CORES * width
    full = width * CORES * deep
    total = experts * cap
    hidden_units = r.wg.shape[1]
    channels, length = r.conv.shape
    heads = channels // HEAD_DIM
    copies = Copies(r.send_sems, r.recv_sems)
    sources = [
        (r.rows_hbm, r.rows), (r.cot_hbm, r.cot), (r.wg_hbm.at[0], r.wg),
        (r.wu_hbm.at[0], r.wu), (r.wd_hbm.at[0], r.wd), (r.conv_hbm, r.conv),
        (r.pre_hbm, r.pre), (r.prior_hbm, r.prior), (r.jump_hbm, r.jump),
        (r.wr_hbm.at[span(tp, heads)], r.wr), (r.wi_hbm.at[span(tp, heads)], r.wi),
        (r.ow_hbm, r.ow),
    ]
    local = [
        pltpu.make_async_copy(a, b, r.local_sems.at[i]) for i, (a, b) in enumerate(sources)
    ]
    for copy in local:
        copy.start()
    greet(planes[1:] + lines[1:] + [partner])
    local[0].wait()
    local[1].wait()
    own = (r.rows, r.cot)
    relieved = (1, 1)
    line = {}
    raw = [(a, d) for a in range(2) for d in range(1, deep) if (a, d) != relieved]
    for a, d in raw:
        line[a, d] = copies.start(own[a], r.held.at[a, d - 1], lines[d])

    expert_ids = lax.broadcasted_iota(jnp.int32, (16, tokens), 0)
    first = r.routes[0:1, :] == expert_ids
    second = r.routes[1:2, :] == expert_ids
    member = (first | second).astype(F32)
    weight_of = jnp.where(first, r.route_w[0:1, :], 0.0) + jnp.where(
        second, r.route_w[1:2, :], 0.0
    )
    earlier = lax.broadcasted_iota(jnp.int32, (tokens, tokens), 0) < lax.broadcasted_iota(
        jnp.int32, (tokens, tokens), 1
    )
    rank = dot(member.astype(BF16), earlier.astype(F32).astype(BF16))
    rank = jnp.where(member > 0.5, rank, -1.0)
    slot_ids = lax.broadcasted_iota(jnp.int32, (cap, tokens), 0).astype(F32)
    for e in range(experts):
        hit = slot_ids == rank[e : e + 1, :]
        r.placing[e * cap : (e + 1) * cap, :] = jnp.where(hit, 1.0, 0.0).astype(BF16)
        r.slot_weight[e * cap : (e + 1) * cap, :] = jnp.sum(
            jnp.where(hit, weight_of[e : e + 1, :], 0.0), axis=1, keepdims=True
        )

    filled = (r.slot_rows, r.slot_cot)
    plane, forward = {}, {}

    def here_of(d):
        return span(levels[d] * CORES + core, width)

    def issue(a, d):
        if (a, d) == relieved:
            return
        if d:
            line[a, d].wait_recv()
        block = r.held[a, d - 1] if d else own[a][...]
        placed = dot(r.placing[...], block)
        if a:
            placed = placed * r.slot_weight[...]
        r.stage[a, d] = placed.astype(BF16)
        for k in range(1, experts):
            plane[a, d, k] = copies.start(
                r.stage.at[a, d, span(planes[k][0], cap)],
                filled[a].at[span(sp, cap), here_of(d)],
                planes[k],
            )
        filled[a][span(sp, cap), here_of(d)] = r.stage[a, d, span(sp, cap), :]

    def pass_on(a, d):
        if (a, d) == relieved:
            line[a, d].wait_recv()
        else:
            for k in range(1, experts):
                plane[a, d, k].wait_recv()
        here = filled[a].at[:, here_of(d)]
        forward[a, d] = copies.start(here, here, partner)
        if d == 0 and a == relieved[0] and deep > 1:
            there = r.slot_cot.at[:, here_of(0)]
            line[relieved] = copies.start(there, there, lines[relieved[1]])

    def row_loop(body):
        size = total // 2

        def step(i, carry):
            body(span(i, size))
            return carry

        lax.fori_loop(0, 2, step, 0)

    seen = [0, 0]

    def absorb(a, d):
        forward[a, d].wait_recv()
        cols = span(levels[d], pair)
        order = seen[a]
        seen[a] += 1
        if a == 0:
            if order == 0:
                local[2].wait()
                local[3].wait()

            def chunk(rows):
                x = r.slot_rows[rows, cols]
                gate = dot(x, r.wg[cols, :])
                up = dot(x, r.wu[cols, :])
                if order:
                    gate = gate + r.acc_gate[rows, :]
                    up = up + r.acc_up[rows, :]
                if order == deep - 1:
                    sigma = jax.nn.sigmoid(gate)
                    silu = gate * sigma
                    r.hidden[rows, :] = (silu * up).astype(BF16)
                    gate = up * (sigma * (1.0 + gate * (1.0 - sigma)))
                    up = silu
                r.acc_gate[rows, :] = gate
                r.acc_up[rows, :] = up
        else:
            if order == 0:
                local[4].wait()

            def chunk(rows):
                value = dot(r.slot_cot[rows, cols], r.wd[:, cols], NT)
                if order:
                    value = value + r.acc_hidden[rows, :]
                if order < deep - 1:
                    r.acc_hidden[rows, :] = value
                else:
                    r.d_gate[rows, :] = (value * r.acc_gate[rows, :]).astype(BF16)
                    r.d_up[rows, :] = (value * r.acc_up[rows, :]).astype(BF16)

        row_loop(chunk)

    eye = lax.broadcasted_iota(jnp.int32, (channels, channels), 0) == lax.broadcasted_iota(
        jnp.int32, (channels, channels), 1
    )
    place = lax.broadcasted_iota(jnp.int32, (channels, length), 1)

    def to_column(row):
        return jnp.sum(jnp.where(eye, row, 0.0), axis=1, keepdims=True)

    def to_row(column):
        return jnp.sum(jnp.where(eye, column, 0.0), axis=0, keepdims=True)

    def by_head(weights, x, dims):
        return jnp.concatenate(
            [
                dot(weights[h], x[h * HEAD_DIM : (h + 1) * HEAD_DIM, :], dims)
                for h in range(heads)
            ],
            axis=0,
        )

    def prepare_gates():
        for i in range(5, 12):
            local[i].wait()
        conv = r.conv[...].astype(F32)
        prior = r.prior[...].astype(F32)
        recur = jax.nn.sigmoid(by_head(r.wr, r.conv[...], TN))
        gate = jax.nn.sigmoid(by_head(r.wi, r.conv[...], TN))
        rate = -r.rate[pl.ds(tp, 1), :]
        soft = to_column(jnp.maximum(rate, 0.0) + log1p_small(jnp.exp(-jnp.abs(rate))))
        log_decay = -RATE_SCALE * recur * soft + r.jump[...]
        decay = jnp.exp(log_decay)
        norm = jnp.sqrt(-expm1_neg(2.0 * log_decay))
        state = decay * prior + norm * gate * conv
        x = r.pre[...].astype(F32)
        inner = 0.7978845608028654 * (x + 0.044715 * (x * x * x))
        bend = jnp.tanh(inner)
        gelu = 0.5 * x * (1.0 + bend)
        slope = 0.5 * (1.0 + bend) + 0.5 * x * (1.0 - bend * bend) * (
            0.7978845608028654 * (1.0 + 3 * 0.044715 * (x * x))
        )
        r.mixed[...] = (gelu * state).astype(BF16)
        pull = prior * decay - gate * conv * decay * decay / norm
        r.keep[0] = pull * (-RATE_SCALE * soft) * recur * (1.0 - recur)
        r.keep[1] = norm * conv * gate * (1.0 - gate)
        r.keep[2] = norm * gate
        r.keep[3] = slope * state
        r.keep[4] = gelu
        r.keep[5] = decay

    def prepare_scan():
        decay = r.keep[5]
        later = jnp.where(place < length - 1, pltpu.roll(decay, length - 1, 1), 1.0)
        reach, level = 1, 0
        while reach < length:
            inside = place < length - reach
            r.reach[level] = jnp.where(inside, later, 0.0)
            later = later * jnp.where(inside, pltpu.roll(later, length - reach, 1), 1.0)
            reach *= 2
            level += 1
        r.keep[6] = later

    def prepare_taking():
        r.taking[...] = r.placing[...].T

    stages = [(0, 0), (1, 0)] + [(0, d) for d in range(1, deep)]
    stages += [(1, d) for d in range(2, deep)]
    stages.insert(len(stages) - 1, relieved)
    between = {1: prepare_gates, 2: prepare_scan, 3: prepare_taking}
    count = len(stages)
    for i in range(count + 2):
        if i < count:
            issue(*stages[i])
        if i in between:
            between[i]()
        if 1 <= i <= count:
            pass_on(*stages[i - 1])
        if i >= 2:
            absorb(*stages[i - 2])

    fillers = []

    def blocks_of(body, steps, group):
        for start in range(0, steps, group):

            def run(start=start):
                def step(i, carry):
                    body(i)
                    return carry

                lax.fori_loop(start, min(start + group, steps), step, 0)

            fillers.append(run)

    wide = 256

    def gate_block(i):
        rows = r.slot_rows[:, span(i, wide)]
        r.gate_grad[0, span(i, wide), :] = dot(rows, r.d_gate[...], TN).astype(BF16)

    def up_block(i):
        rows = r.slot_rows[:, span(i, wide)]
        r.up_grad[0, span(i, wide), :] = dot(rows, r.d_up[...], TN).astype(BF16)

    def down_block(i):
        cols = span(i, wide)
        r.down_grad[0, :, cols] = dot(r.hidden[...], r.slot_cot[:, cols], TN).astype(BF16)

    blocks_of(down_block, full // wide, 2)
    blocks_of(gate_block, full // wide, 2)
    blocks_of(up_block, full // wide, 2)

    def fill(amount):
        for _ in range(amount):
            if fillers:
                fillers.pop(0)()

    order = list(range(deep - 1, -1, -1))
    core_copy, home_copy, line_copy = {}, {}, {}

    def width_block(block, store):
        def chunk(rows):
            value = dot(r.d_gate[rows, :], r.wg[span(block, width), :], NT)
            store(rows, value + dot(r.d_up[rows, :], r.wu[span(block, width), :], NT))

        row_loop(chunk)

    def theirs(d):
        def store(rows, value):
            r.lent[d, rows, :] = value.astype(BF16)

        width_block(levels[d] * CORES + 1 - core, store)
        core_copy[d] = copies.start(r.lent.at[d], r.paired.at[d], partner)

    def mine(d):
        def store(rows, value):
            r.kept[d, rows, :] = value

        width_block(levels[d] * CORES + core, store)

    def ship(d):
        core_copy[d].wait_recv()
        r.joint[d] = (r.kept[d] + r.paired[d].astype(F32)).astype(BF16)
        for k in range(1, experts):
            home_copy[d, k] = copies.start(
                r.joint.at[d, span(planes[k][0], cap)],
                r.homed.at[d, span(sp, cap)],
                planes[k],
            )
        r.homed[d, span(sp, cap), :] = r.joint[d, span(sp, cap), :]

    theirs(order[0])
    for i, d in enumerate(order):
        mine(d)
        if i + 1 < deep:
            theirs(order[i + 1])
        ship(d)
    fill(1)
    for d in order:
        for k in range(1, experts):
            home_copy[d, k].wait_recv()
        summed = dot(r.taking[...], r.homed[d])
        if d:
            r.line_out[d - 1] = summed.astype(BF16)
            line_copy[d] = copies.start(r.line_out.at[d - 1], r.line_in.at[d - 1], lines[d])
        else:
            r.sum_own[...] = summed + r.cot[...].astype(F32)
        fill(2)
    value = r.sum_own[...]
    for d in order[:-1]:
        line_copy[d].wait_recv()
        value = value + r.line_in[d - 1].astype(F32)
    here = span(tp, width)
    r.block_grad[:, here] = value.astype(BF16)
    gathers, shared = {}, {}
    for d in range(1, deep):
        gathers[d] = copies.start(
            r.block_grad.at[:, here], r.block_grad.at[:, here], lines[d]
        )
    shared[0] = copies.start(r.block_grad.at[:, here], r.block_grad.at[:, here], partner)
    fill(2)

    def level_done(d):
        shared[d].wait_recv()
        cols = span(levels[d], pair)
        block = r.block_grad[:, cols]
        r.product[:, cols] = dot(r.mixed[...], block).astype(BF16)
        value = dot(r.ow[:, cols], block, NT)
        r.d_mixed[...] = value if d == 0 else r.d_mixed[...] + value

    level_done(0)
    for d in range(1, deep):
        fill(2)
        gathers[d].wait_recv()
        spot = r.block_grad.at[:, here_of(d)]
        shared[d] = copies.start(spot, spot, partner)
        if d == deep - 1:
            fill(100)
        if d > 1:
            level_done(d - 1)
    level_done(deep - 1)

    d_mixed = r.d_mixed[...]
    value = d_mixed * r.keep[4]
    reach, level = 1, 0
    while reach < length:
        value = value + r.reach[level] * pltpu.roll(value, length - reach, 1)
        reach *= 2
        level += 1
    decay_first = r.keep[5][:, 0:1]
    head_prod = to_row(decay_first * r.keep[6][:, 0:1])
    head_sum = to_row(decay_first * value[:, 0:1])
    r.summary[0:1, :] = head_prod
    r.summary[1:2, :] = head_sum
    tails = []
    for k in range(1, experts):
        tails.append(copies.start(r.summary, r.summaries.at[sp], planes[k]))
    out_width = r.products.shape[2]
    for k in range(1, experts):
        tails.append(
            copies.start(
                r.product.at[:, span(planes[k][0], out_width)], r.products.at[k - 1], planes[k]
            )
        )
    r.summaries[sp] = r.summary[...]
    r.valve[...] = (d_mixed * r.keep[3]).astype(BF16)
    for copy in tails[: experts - 1]:
        copy.wait_recv()
    carried = jnp.zeros((1, channels), F32)
    for later in range(experts - 1, 0, -1):
        longer = r.summaries[later, 1:2, :] + r.summaries[later, 0:1, :] * carried
        carried = jnp.where(later > sp, longer, carried)
    state_grad = value + r.keep[6] * to_column(carried)
    grad_recur = (state_grad * r.keep[0]).astype(BF16)
    grad_input = (state_grad * r.keep[1]).astype(BF16)
    conv_grad = state_grad * r.keep[2]
    conv_grad = conv_grad + by_head(r.wr, grad_recur, NN) + by_head(r.wi, grad_input, NN)
    r.conv_grad[...] = conv_grad.astype(BF16)
    value = r.product[:, span(sp, out_width)].astype(F32)
    for k in range(1, experts):
        tails[experts - 2 + k].wait_recv()
        value = value + r.products[k - 1].astype(F32)
    r.out_grad[...] = value
    for copy in copies.sent:
        copy.wait_send()


def local(
    cotangent,
    block_input,
    routes,
    route_weights,
    gate_weight,
    up_weight,
    down_weight,
    out_weight,
    conv_out,
    gate_pre,
    prior_states,
    recur_weight,
    input_gate_matrix,
    decay_param,
    decay_jump,
):
    experts, columns = lax.axis_size("sp"), lax.axis_size("tp")
    deep = columns // CORES
    tokens, width = cotangent.shape
    cap = -(-(5 * tokens * TOP_K // (4 * experts)) // 16) * 16
    total = experts * cap
    full = width * columns
    units = gate_weight.shape[2]
    channels, length = conv_out.shape
    heads = channels // HEAD_DIM
    doublings = (length - 1).bit_length()
    copies = 2 * deep * (experts + 1) + 2 * deep + deep * (experts + 3) + 2 * experts
    vmem = pltpu.VMEM
    scratch = dict(
        rows=vmem((tokens, width), BF16),
        cot=vmem((tokens, width), BF16),
        wg=vmem((full, units), BF16),
        wu=vmem((full, units), BF16),
        wd=vmem((units, full), BF16),
        ow=vmem((channels, full), BF16),
        conv=vmem((channels, length), BF16),
        pre=vmem((channels, length), BF16),
        prior=vmem((channels, length), BF16),
        jump=vmem((channels, length), F32),
        wr=vmem((heads, HEAD_DIM, HEAD_DIM), BF16),
        wi=vmem((heads, HEAD_DIM, HEAD_DIM), BF16),
        held=vmem((2, deep - 1, tokens, width), BF16),
        placing=vmem((total, tokens), BF16),
        taking=vmem((tokens, total), BF16),
        slot_weight=vmem((total, 1), F32),
        stage=vmem((2, deep, total, width), BF16),
        slot_rows=vmem((total, full), BF16),
        slot_cot=vmem((total, full), BF16),
        acc_gate=vmem((total, units), F32),
        acc_up=vmem((total, units), F32),
        acc_hidden=vmem((total, units), F32),
        hidden=vmem((total, units), BF16),
        d_gate=vmem((total, units), BF16),
        d_up=vmem((total, units), BF16),
        lent=vmem((deep, total, width), BF16),
        paired=vmem((deep, total, width), BF16),
        kept=vmem((deep, total, width), F32),
        joint=vmem((deep, total, width), BF16),
        homed=vmem((deep, total, width), BF16),
        line_out=vmem((deep - 1, tokens, width), BF16),
        line_in=vmem((deep - 1, tokens, width), BF16),
        sum_own=vmem((tokens, width), F32),
        block_grad=vmem((tokens, full), BF16),
        mixed=vmem((channels, length), BF16),
        d_mixed=vmem((channels, length), F32),
        keep=vmem((7, channels, length), F32),
        reach=vmem((doublings, channels, length), F32),
        product=vmem((channels, full), BF16),
        products=vmem((experts - 1, channels, full // experts), BF16),
        summary=vmem((8, channels), F32),
        summaries=vmem((experts, 8, channels), F32),
        send_sems=pltpu.SemaphoreType.DMA((copies,)),
        recv_sems=pltpu.SemaphoreType.DMA((copies,)),
        local_sems=pltpu.SemaphoreType.DMA((12,)),
    )
    on_chip = pl.BlockSpec(memory_space=pltpu.VMEM)
    far = pl.BlockSpec(memory_space=pltpu.HBM)
    given = ("routes", "route_w", "rate")
    return pl.pallas_call(
        functools.partial(kernel, INPUTS + OUTPUTS + tuple(scratch), experts, deep, cap),
        out_shape=(
            jax.ShapeDtypeStruct(gate_weight.shape, BF16),
            jax.ShapeDtypeStruct(up_weight.shape, BF16),
            jax.ShapeDtypeStruct(down_weight.shape, BF16),
            jax.ShapeDtypeStruct((channels, full // experts), F32),
            jax.ShapeDtypeStruct((channels, length), BF16),
            jax.ShapeDtypeStruct((channels, length), BF16),
        ),
        in_specs=[on_chip if name in given else far for name in INPUTS],
        out_specs=(on_chip,) * 6,
        scratch_shapes=list(scratch.values()),
        compiler_params=pltpu.CompilerParams(
            collective_id=0, has_side_effects=True, vmem_limit_bytes=67043328
        ),
    )(
        block_input,
        cotangent,
        jnp.transpose(routes),
        jnp.transpose(route_weights),
        gate_weight,
        up_weight,
        down_weight,
        out_weight,
        conv_out,
        gate_pre,
        prior_states,
        recur_weight,
        input_gate_matrix,
        decay_param.reshape(columns, channels),
        decay_jump,
    )


def solution(mesh):
    in_specs = (
        P("sp", "tp"),
        P("sp", "tp"),
        P("sp", None),
        P("sp", None),
        P("sp", None, "tp"),
        P("sp", None, "tp"),
        P("sp", "tp", None),
        P("tp", None),
        P("tp", "sp"),
        P("tp", "sp"),
        P("tp", "sp"),
        P(),
        P(),
        P(),
        P("tp", "sp"),
    )
    out_specs = (
        P("sp", None, "tp"),
        P("sp", None, "tp"),
        P("sp", "tp", None),
        P("tp", "sp"),
        P("tp", "sp"),
        P("tp", "sp"),
    )
    return jax.shard_map(local, mesh=mesh, in_specs=in_specs, out_specs=out_specs, check_vma=False)
```

time: 146 us -> 107 us (0.73)
  matrix products: 42.2 us -> 0 us
  Pallas kernels: 86.7 us -> 94.2 us
  other arithmetic: 5.45 us -> 0 us
  local copies, waits for them, and re-layouts: 9.39 us -> 11.5 us
    dot_general x14 -> x0, matrix products: 42.2 us -> none  [the longest x1 7.39 us: weight_grads(): lax.dot_general(slot_rows, d_up, major, preferred_element_type=jnp.float32)]
    pallas_call x3 -> x1, Pallas kernels: 86.7 us -> 94.2 us  [local(): pl.pallas_call(functools.partial(kernel, INPUTS + OUTPUTS + tuple(scratch...]
    unnamed x53 -> x16, local copies, waits for them, and re-layouts: 6.42 us -> 11.5 us
    reduce_sum x3 -> x0, other arithmetic: 1.81 us -> none  [the longest x1 1.01 us: local(): jnp.sum(jnp.where(route_hits, jnp.transpose(route_weights)[:, None, :], 0...]
where the time goes in v1:
time: 107 us; the launch traced here: 106 us
  Pallas kernels  94.2 us (88%)
  local copies, waits for them, and re-layouts  11.5 us (11%)
    pallas_call x1, Pallas kernels, local(): pl.pallas_call(functools.partial(kernel, INPUTS + OUTPUTS + tuple(scratch...  94.2 us
    unnamed x16, local copies, waits for them, and re-layouts  11.5 us

profile of v1, /device:TPU:0, one launch (start us, length us, event | category | flops | bytes accessed | tf_op | source)
XLA Modules:
  0.0 106.3 jit_solution(3790768674621584247)
XLA Ops:
  0.6 94.2 %shard_map.190 = (bf16[1,2048,896]{2,1,0:T(8,128)(2,1)}, bf16[1,2048,896]{2,1,0:T(8,128)(2,1)}, bf16[1,896,2048]{2,1,0:T(8,128)(2,1)}, f32[128,512]{1,0:T(8,128)...) custom-call(bf16[256,256]{1,0:T(8,128)(2,1)} %refs_0_.1, bf16[256,256]{1,0:T(8,128)(2,1)} %refs_1_.1, ...), custom_call_target="tpu_custom_call" | custom-call | tf_op jit(solution)/shard_map/pallas_call | solution.py:564
  94.8 0.0 copy-start.1
  94.9 4.3 %copy.27 = bf16[1,2048,896]{2,1,0:T(8,128)(2,1)} copy(bf16[1,2048,896]{2,1,0:T(8,128)(2,1)} %get-tuple-element.12) | data formatting | bytes 7340032
  99.2 0.0 copy-done.1
  99.2 0.0 copy-start
  99.2 1.9 %copy.28 = bf16[1,2048,896]{2,1,0:T(8,128)(2,1)} copy(bf16[1,2048,896]{2,1,0:T(8,128)(2,1)S(1)} %copy-done.1) | data formatting | bytes 7340032
  101.0 1.5 %copy-done = bf16[1,896,2048]{2,1,0:T(8,128)(2,1)S(1)} copy-done((bf16[1,896,2048]{2,1,0:T(8,128)(2,1)S(1)}, bf16[1,896,2048]{2,1,0:T(8,128)(2,1)}, u32[]{:S(2)}) %copy-start) | copy-done | bytes 3670040
  102.5 0.0 copy-start.2
  102.5 0.0 copy-start.4
  102.5 0.0 copy-start.3
  102.5 1.8 %copy.29 = bf16[1,896,2048]{2,1,0:T(8,128)(2,1)} copy(bf16[1,896,2048]{2,1,0:T(8,128)(2,1)S(1)} %copy-done) | data formatting | bytes 7340032
  104.4 0.0 copy-done.2
  104.4 0.7 copy.30
  105.1 0.0 copy-done.4
  105.1 0.6 copy.31
  105.7 0.0 copy-done.3
  105.7 0.6 copy.32
Async XLA Ops:
  94.8 4.3 %copy-start.1 = (bf16[1,2048,896]{2,1,0:T(8,128)(2,1)S(1)}, bf16[1,2048,896]{2,1,0:T(8,128)(2,1)}, u32[]{:S(2)}) copy-start(bf16[1,2048,896]{2,1,0:T(8,128)(2,1)} %get-tuple-element.13) | copy-start | bytes 11010052
  99.2 3.4 %copy-start = (bf16[1,896,2048]{2,1,0:T(8,128)(2,1)S(1)}, bf16[1,896,2048]{2,1,0:T(8,128)(2,1)}, u32[]{:S(2)}) copy-start(bf16[1,896,2048]{2,1,0:T(8,128)(2,1)} %get-tuple-element.14) | copy-start | bytes 11010052
  102.5 1.8 %copy-start.2 = (f32[128,512]{1,0:T(8,128)S(1)}, f32[128,512]{1,0:T(8,128)}, u32[]{:S(2)}) copy-start(f32[128,512]{1,0:T(8,128)} %get-tuple-element.15) | copy-start | bytes 786436
  102.5 2.5 %copy-start.4 = (bf16[128,256]{1,0:T(8,128)(2,1)S(1)}, bf16[128,256]{1,0:T(8,128)(2,1)}, u32[]{:S(2)}) copy-start(bf16[128,256]{1,0:T(8,128)(2,1)} %get-tuple-element.16) | copy-start | bytes 196612
  102.5 3.2 %copy-start.3 = (bf16[128,256]{1,0:T(8,128)(2,1)S(1)}, bf16[128,256]{1,0:T(8,128)(2,1)}, u32[]{:S(2)}) copy-start(bf16[128,256]{1,0:T(8,128)(2,1)} %get-tuple-element.17) | copy-start | bytes 196612

commit v2 on v1

--- a/solution.py
+++ b/solution.py
@@ -34,13 +34,12 @@
     return pl.ds(pl.multiple_of(block * width, width), width)
 
 
-def greet(devices):
+def signal(devices):
     barrier = pltpu.get_barrier_semaphore()
     for device in devices:
         pl.semaphore_signal(
             barrier, inc=1, device_id=device, device_id_type=pl.DeviceIdType.MESH
         )
-    pl.semaphore_wait(barrier, len(devices))
 
 
 def log1p_small(y):
@@ -62,19 +61,30 @@
         self.count = 0
         self.sent = []
 
-    def start(self, source, target, device):
+    def start(self, source, target, device, when=None, arrival=None):
+        index, self.count = self.count, self.count + 1
         copy = pltpu.make_async_remote_copy(
             src_ref=source,
             dst_ref=target,
-            send_sem=self.sems[0].at[self.count],
-            recv_sem=self.sems[1].at[self.count],
+            send_sem=self.sems[0].at[index],
+            recv_sem=self.sems[1].at[index if arrival is None else arrival],
             device_id=device,
             device_id_type=pl.DeviceIdType.MESH,
         )
-        copy.start()
-        self.count += 1
-        self.sent.append(copy)
-        return copy
+        self.run(when, copy.start)
+        self.sent.append((when, copy))
+        return index, copy
+
+    def run(self, when, action):
+        if when is None:
+            action()
+        else:
+            pl.when(when)(action)
+
+    def finish(self):
+        for when, copy in self.sent:
+            self.run(when, copy.wait_send)
+        self.sent = []
 
 
 INPUTS = (
@@ -116,17 +126,24 @@
     local = [
         pltpu.make_async_copy(a, b, r.local_sems.at[i]) for i, (a, b) in enumerate(sources)
     ]
+    peers = planes[1:] + lines[1:] + [partner]
+    signal(peers)
     for copy in local:
         copy.start()
-    greet(planes[1:] + lines[1:] + [partner])
+    with jax.named_scope("greet"):
+        pl.semaphore_wait(pltpu.get_barrier_semaphore(), len(peers))
     local[0].wait()
     local[1].wait()
     own = (r.rows, r.cot)
     relieved = (1, 1)
+    relay = deep == 4
+    middle = (z == 1) | (z == 2)
     line = {}
     raw = [(a, d) for a in range(2) for d in range(1, deep) if (a, d) != relieved]
     for a, d in raw:
-        line[a, d] = copies.start(own[a], r.held.at[a, d - 1], lines[d])
+        line[a, d] = copies.start(
+            own[a], r.held.at[a, d - 1], lines[d], middle if relay and d == 3 else None
+        )
 
     expert_ids = lax.broadcasted_iota(jnp.int32, (16, tokens), 0)
     first = r.routes[0:1, :] == expert_ids
@@ -155,10 +172,12 @@
         return span(levels[d] * CORES + core, width)
 
     def issue(a, d):
-        if (a, d) == relieved:
-            return
         if d:
-            line[a, d].wait_recv()
+            line[a, d][1].wait_recv()
+        if relay and d == 2:
+            copies.start(
+                r.held.at[a, 1], r.held.at[a, 2], lines[1], middle, line[a, 3][0]
+            )
         block = r.held[a, d - 1] if d else own[a][...]
         placed = dot(r.placing[...], block)
         if a:
@@ -169,7 +188,7 @@
                 r.stage.at[a, d, span(planes[k][0], cap)],
                 filled[a].at[span(sp, cap), here_of(d)],
                 planes[k],
-            )
+            )[1]
         filled[a][span(sp, cap), here_of(d)] = r.stage[a, d, span(sp, cap), :]
 
     def pass_on(a, d):
@@ -179,10 +198,10 @@
             for k in range(1, experts):
                 plane[a, d, k].wait_recv()
         here = filled[a].at[:, here_of(d)]
-        forward[a, d] = copies.start(here, here, partner)
-        if d == 0 and a == relieved[0] and deep > 1:
+        forward[a, d] = copies.start(here, here, partner)[1]
+        if d == 0 and a == relieved[0]:
             there = r.slot_cot.at[:, here_of(0)]
-            line[relieved] = copies.start(there, there, lines[relieved[1]])
+            line[relieved] = copies.start(there, there, lines[relieved[1]])[1]
 
     def row_loop(body):
         size = total // 2
@@ -300,20 +319,31 @@
     def prepare_taking():
         r.taking[...] = r.placing[...].T
 
+    def scoped(name, fn, *args):
+        with jax.named_scope(name):
+            fn(*args)
+
     stages = [(0, 0), (1, 0)] + [(0, d) for d in range(1, deep)]
     stages += [(1, d) for d in range(2, deep)]
-    stages.insert(len(stages) - 1, relieved)
-    between = {1: prepare_gates, 2: prepare_scan, 3: prepare_taking}
+    between = {0: prepare_gates, 1: prepare_scan, 2: prepare_taking}
+    scoped("issue", issue, *stages[0])
+    scoped("issue", issue, *stages[1])
     count = len(stages)
-    for i in range(count + 2):
-        if i < count:
-            issue(*stages[i])
+    behind = []
+    for i in range(count):
         if i in between:
-            between[i]()
-        if 1 <= i <= count:
-            pass_on(*stages[i - 1])
-        if i >= 2:
-            absorb(*stages[i - 2])
+            scoped("between", between[i])
+        if i + 2 < count:
+            scoped(f"issue#i={i + 2}", issue, *stages[i + 2])
+        if i == count - 1:
+            scoped("pass_on_relieved", pass_on, *relieved)
+            scoped("absorb_relieved", absorb, *stages[i - 1])
+            behind = [relieved]
+        elif i:
+            scoped(f"absorb#i={i - 1}", absorb, *stages[i - 1])
+        scoped(f"pass_on#i={i}", pass_on, *stages[i])
+    for stage in behind + [stages[-1]]:
+        scoped("absorb_last", absorb, *stage)
 
     fillers = []
 
@@ -350,92 +380,153 @@
     def fill(amount):
         for _ in range(amount):
             if fillers:
-                fillers.pop(0)()
-
+                scoped("fill", fillers.pop(0))
+
+    halves = max(1, width // 128)
+    half = width // halves
     order = list(range(deep - 1, -1, -1))
     core_copy, home_copy, line_copy = {}, {}, {}
 
-    def width_block(block, store):
+    def kept_of(d, start, size):
+        room = hidden_units // width
+        first = d % room * width + start
+        return (r.acc_gate, r.acc_up, r.acc_hidden)[d // room], slice(first, first + size)
+
+    def pair_block(d):
         def chunk(rows):
-            value = dot(r.d_gate[rows, :], r.wg[span(block, width), :], NT)
-            store(rows, value + dot(r.d_up[rows, :], r.wu[span(block, width), :], NT))
+            gate, up = r.d_gate[rows, :], r.d_up[rows, :]
+            for which, block in enumerate((levels[d] * CORES + 1 - core, levels[d] * CORES + core)):
+                value = dot(gate, r.wg[span(block, width), :], NT)
+                value = value + dot(up, r.wu[span(block, width), :], NT)
+                if which:
+                    kept, cols = kept_of(d, 0, width)
+                    kept[rows, cols] = value
+                else:
+                    r.stage[0, d, rows, :] = value.astype(BF16)
 
         row_loop(chunk)
-
-    def theirs(d):
-        def store(rows, value):
-            r.lent[d, rows, :] = value.astype(BF16)
-
-        width_block(levels[d] * CORES + 1 - core, store)
-        core_copy[d] = copies.start(r.lent.at[d], r.paired.at[d], partner)
-
-    def mine(d):
-        def store(rows, value):
-            r.kept[d, rows, :] = value
-
-        width_block(levels[d] * CORES + core, store)
-
-    def ship(d):
-        core_copy[d].wait_recv()
-        r.joint[d] = (r.kept[d] + r.paired[d].astype(F32)).astype(BF16)
+        core_copy[d] = copies.start(r.stage.at[0, d], r.paired.at[d], partner)[1]
+
+    def ship(d, h):
+        if h == 0:
+            core_copy[d].wait_recv()
+        cols = slice(h * half, (h + 1) * half)
+        kept, kept_cols = kept_of(d, h * half, half)
+        joint = kept[:, kept_cols] + r.paired[d, :, cols].astype(F32)
+        r.stage[1, d, :, cols] = joint.astype(BF16)
         for k in range(1, experts):
-            home_copy[d, k] = copies.start(
-                r.joint.at[d, span(planes[k][0], cap)],
-                r.homed.at[d, span(sp, cap)],
+            home_copy[d, h, k] = copies.start(
+                r.stage.at[1, d, span(planes[k][0], cap), pl.ds(h * half, half)],
+                r.homed.at[h, d, span(sp, cap)],
                 planes[k],
+            )[1]
+        r.homed[h, d, span(sp, cap), :] = r.stage[1, d, span(sp, cap), cols]
+
+    def home(d, h):
+        for k in range(1, experts):
+            home_copy[d, h, k].wait_recv()
+        summed = dot(r.taking[...], r.homed[h, d])
+        if d:
+            r.line_out[h, d - 1] = summed.astype(BF16)
+            line_copy[d, h] = copies.start(
+                r.line_out.at[h, d - 1], r.line_in.at[h, d - 1], lines[d]
+            )[1]
+        else:
+            cols = slice(h * half, (h + 1) * half)
+            r.sum_own[h] = summed + r.cot[:, cols].astype(F32)
+
+    def spot_of(place_of, h):
+        return r.block_grad.at[:, span(place_of * halves + h, half)]
+
+    gathers, shared = {}, {}
+
+    def close_sum(h):
+        value = r.sum_own[h]
+        for d in order[:-1]:
+            line_copy[d, h].wait_recv()
+            value = value + r.line_in[h, d - 1].astype(F32)
+        r.block_grad[:, span(tp * halves + h, half)] = value.astype(BF16)
+        spot = spot_of(tp, h)
+        for d in range(1, deep):
+            gathers[d, h] = copies.start(
+                spot, spot, lines[d], middle if relay and d == 3 else None
             )
-        r.homed[d, span(sp, cap), :] = r.joint[d, span(sp, cap), :]
-
-    theirs(order[0])
+        shared[0, h] = copies.start(spot, spot, partner)[1]
+
+    def gather(d, h):
+        gathers[d, h][1].wait_recv()
+        spot = spot_of(levels[d] * CORES + core, h)
+        if relay and d == 2:
+            copies.start(spot, spot, lines[1], middle, gathers[3, h][0])
+        shared[d, h] = copies.start(spot, spot, partner)[1]
+
+    share = (full // experts) // width
+    pieces = {}
+
+    def arrival_of(slot, q, h):
+        return r.piece_sems.at[(slot * share + q) * halves + h]
+
+    def use(d, h):
+        shared[d, h].wait_recv()
+        for c in range(CORES):
+            block = levels[d] * CORES + c
+            cols = span(block * halves + h, half)
+            grads = r.block_grad[:, cols]
+            value = dot(r.ow[:, cols], grads, NT)
+            start = d == 0 and h == 0 and c == 0
+            r.d_mixed[...] = value if start else r.d_mixed[...] + value
+            r.product[d, h, c] = dot(r.mixed[...], grads).astype(BF16)
+            to, q = lax.div(block, share), lax.rem(block, share)
+            copy = pltpu.make_async_remote_copy(
+                src_ref=r.product.at[d, h, c],
+                dst_ref=r.products.at[sp, q, h],
+                send_sem=r.sent_sems.at[(d * halves + h) * CORES + c],
+                recv_sem=arrival_of(sp, q, h),
+                device_id=(to, tp),
+                device_id_type=pl.DeviceIdType.MESH,
+            )
+            pl.when(to != sp)(copy.start)
+            copies.sent.append((to != sp, copy))
+
+            @pl.when(to == sp)
+            def _():
+                r.products[sp, q, h] = r.product[d, h, c]
+
+    with jax.named_scope("settle"):
+        copies.finish()
+    scoped("pair", pair_block, order[0])
     for i, d in enumerate(order):
-        mine(d)
         if i + 1 < deep:
-            theirs(order[i + 1])
-        ship(d)
-    fill(1)
-    for d in order:
-        for k in range(1, experts):
-            home_copy[d, k].wait_recv()
-        summed = dot(r.taking[...], r.homed[d])
-        if d:
-            r.line_out[d - 1] = summed.astype(BF16)
-            line_copy[d] = copies.start(r.line_out.at[d - 1], r.line_in.at[d - 1], lines[d])
-        else:
-            r.sum_own[...] = summed + r.cot[...].astype(F32)
-        fill(2)
-    value = r.sum_own[...]
-    for d in order[:-1]:
-        line_copy[d].wait_recv()
-        value = value + r.line_in[d - 1].astype(F32)
-    here = span(tp, width)
-    r.block_grad[:, here] = value.astype(BF16)
-    gathers, shared = {}, {}
+            scoped("pair", pair_block, order[i + 1])
+        scoped("ship", ship, d, 0)
+    for h in range(1, halves):
+        for d in order:
+            scoped("ship", ship, d, h)
+    for h in range(halves):
+        for i, d in enumerate(order):
+            fill(1)
+            scoped(f"home#h={h}#d={d}", home, d, h)
+            if h and i == 0:
+                scoped("sum", close_sum, h - 1)
+            if h and i == 2:
+                scoped("gather", gather, 1, h - 1)
+            if h and i == 3:
+                scoped("gather", gather, 2, h - 1)
+                for e in range(3, deep):
+                    scoped("gather", gather, e, h - 1)
+                for e in range(2):
+                    scoped("use", use, e, h - 1)
+    scoped("sum", close_sum, halves - 1)
+    for h in range(halves - 1):
+        for d in range(2, deep):
+            scoped("use", use, d, h)
+    fill(100)
+    scoped("use", use, 0, halves - 1)
     for d in range(1, deep):
-        gathers[d] = copies.start(
-            r.block_grad.at[:, here], r.block_grad.at[:, here], lines[d]
-        )
-    shared[0] = copies.start(r.block_grad.at[:, here], r.block_grad.at[:, here], partner)
-    fill(2)
-
-    def level_done(d):
-        shared[d].wait_recv()
-        cols = span(levels[d], pair)
-        block = r.block_grad[:, cols]
-        r.product[:, cols] = dot(r.mixed[...], block).astype(BF16)
-        value = dot(r.ow[:, cols], block, NT)
-        r.d_mixed[...] = value if d == 0 else r.d_mixed[...] + value
-
-    level_done(0)
-    for d in range(1, deep):
-        fill(2)
-        gathers[d].wait_recv()
-        spot = r.block_grad.at[:, here_of(d)]
-        shared[d] = copies.start(spot, spot, partner)
-        if d == deep - 1:
-            fill(100)
+        scoped("gather", gather, d, halves - 1)
         if d > 1:
-            level_done(d - 1)
-    level_done(deep - 1)
+            scoped("use", use, d - 1, halves - 1)
+    scoped("use", use, deep - 1, halves - 1)
 
     d_mixed = r.d_mixed[...]
     value = d_mixed * r.keep[4]
@@ -445,24 +536,16 @@
         reach *= 2
         level += 1
     decay_first = r.keep[5][:, 0:1]
-    head_prod = to_row(decay_first * r.keep[6][:, 0:1])
-    head_sum = to_row(decay_first * value[:, 0:1])
-    r.summary[0:1, :] = head_prod
-    r.summary[1:2, :] = head_sum
+    r.summary[0:1, :] = to_row(decay_first * r.keep[6][:, 0:1])
+    r.summary[1:2, :] = to_row(decay_first * value[:, 0:1])
     tails = []
     for k in range(1, experts):
-        tails.append(copies.start(r.summary, r.summaries.at[sp], planes[k]))
-    out_width = r.products.shape[2]
-    for k in range(1, experts):
-        tails.append(
-            copies.start(
-                r.product.at[:, span(planes[k][0], out_width)], r.products.at[k - 1], planes[k]
-            )
-        )
+        tails.append(copies.start(r.summary, r.summaries.at[sp], planes[k])[1])
     r.summaries[sp] = r.summary[...]
     r.valve[...] = (d_mixed * r.keep[3]).astype(BF16)
-    for copy in tails[: experts - 1]:
-        copy.wait_recv()
+    with jax.named_scope("summaries"):
+        for copy in tails:
+            copy.wait_recv()
     carried = jnp.zeros((1, channels), F32)
     for later in range(experts - 1, 0, -1):
         longer = r.summaries[later, 1:2, :] + r.summaries[later, 0:1, :] * carried
@@ -473,13 +556,37 @@
     conv_grad = state_grad * r.keep[2]
     conv_grad = conv_grad + by_head(r.wr, grad_recur, NN) + by_head(r.wi, grad_input, NN)
     r.conv_grad[...] = conv_grad.astype(BF16)
-    value = r.product[:, span(sp, out_width)].astype(F32)
-    for k in range(1, experts):
-        tails[experts - 2 + k].wait_recv()
-        value = value + r.products[k - 1].astype(F32)
-    r.out_grad[...] = value
-    for copy in copies.sent:
-        copy.wait_send()
+    with jax.named_scope("products"):
+        for k in range(1, experts):
+            for q in range(share):
+                for h in range(halves):
+                    spot = r.products.at[planes[k][0], q, h]
+                    pltpu.make_async_remote_copy(
+                        src_ref=r.product.at[0, 0, 0],
+                        dst_ref=spot,
+                        send_sem=r.sent_sems.at[0],
+                        recv_sem=arrival_of(planes[k][0], q, h),
+                        device_id=planes[k],
+                        device_id_type=pl.DeviceIdType.MESH,
+                    ).wait_recv()
+    for q in range(share):
+        for h in range(halves):
+            value = r.products[0, q, h].astype(F32)
+            for e in range(1, experts):
+                value = value + r.products[e, q, h].astype(F32)
+            r.out_grad[:, q * width + h * half : q * width + (h + 1) * half] = value
+    copies.finish()
+
+
+def export_kernel(*refs):
+    count = (len(refs) - 1) // 2
+    copies = [
+        pltpu.make_async_copy(refs[i], refs[count + i], refs[-1].at[i]) for i in range(count)
+    ]
+    for copy in copies:
+        copy.start()
+    for copy in copies:
+        copy.wait()
 
 
 def local(
@@ -509,7 +616,10 @@
     channels, length = conv_out.shape
     heads = channels // HEAD_DIM
     doublings = (length - 1).bit_length()
-    copies = 2 * deep * (experts + 1) + 2 * deep + deep * (experts + 3) + 2 * experts
+    halves = max(1, width // 128)
+    half = width // halves
+    share = (full // experts) // width
+    copies = 2 * deep * (experts + 2) + deep + halves * deep * (experts + 4) + experts
     vmem = pltpu.VMEM
     scratch = dict(
         rows=vmem((tokens, width), BF16),
@@ -537,63 +647,74 @@
         hidden=vmem((total, units), BF16),
         d_gate=vmem((total, units), BF16),
         d_up=vmem((total, units), BF16),
-        lent=vmem((deep, total, width), BF16),
         paired=vmem((deep, total, width), BF16),
-        kept=vmem((deep, total, width), F32),
-        joint=vmem((deep, total, width), BF16),
-        homed=vmem((deep, total, width), BF16),
-        line_out=vmem((deep - 1, tokens, width), BF16),
-        line_in=vmem((deep - 1, tokens, width), BF16),
-        sum_own=vmem((tokens, width), F32),
+        homed=vmem((halves, deep, total, half), BF16),
+        line_out=vmem((halves, deep - 1, tokens, half), BF16),
+        line_in=vmem((halves, deep - 1, tokens, half), BF16),
+        sum_own=vmem((halves, tokens, half), F32),
         block_grad=vmem((tokens, full), BF16),
         mixed=vmem((channels, length), BF16),
         d_mixed=vmem((channels, length), F32),
         keep=vmem((7, channels, length), F32),
         reach=vmem((doublings, channels, length), F32),
-        product=vmem((channels, full), BF16),
-        products=vmem((experts - 1, channels, full // experts), BF16),
+        product=vmem((deep, halves, CORES, channels, half), BF16),
+        products=vmem((experts, share, halves, channels, half), BF16),
         summary=vmem((8, channels), F32),
         summaries=vmem((experts, 8, channels), F32),
         send_sems=pltpu.SemaphoreType.DMA((copies,)),
         recv_sems=pltpu.SemaphoreType.DMA((copies,)),
         local_sems=pltpu.SemaphoreType.DMA((12,)),
+        sent_sems=pltpu.SemaphoreType.DMA((deep * halves * CORES,)),
+        piece_sems=pltpu.SemaphoreType.DMA((experts * share * halves,)),
     )
     on_chip = pl.BlockSpec(memory_space=pltpu.VMEM)
     far = pl.BlockSpec(memory_space=pltpu.HBM)
     given = ("routes", "route_w", "rate")
-    return pl.pallas_call(
+
+    def in_hbm(x):
+        return pltpu.with_memory_space_constraint(x, pltpu.HBM)
+
+    results = pl.pallas_call(
         functools.partial(kernel, INPUTS + OUTPUTS + tuple(scratch), experts, deep, cap),
         out_shape=(
-            jax.ShapeDtypeStruct(gate_weight.shape, BF16),
-            jax.ShapeDtypeStruct(up_weight.shape, BF16),
-            jax.ShapeDtypeStruct(down_weight.shape, BF16),
-            jax.ShapeDtypeStruct((channels, full // experts), F32),
-            jax.ShapeDtypeStruct((channels, length), BF16),
-            jax.ShapeDtypeStruct((channels, length), BF16),
+            vmem(gate_weight.shape, BF16),
+            vmem(up_weight.shape, BF16),
+            vmem(down_weight.shape, BF16),
+            vmem((channels, full // experts), F32),
+            vmem((channels, length), BF16),
+            vmem((channels, length), BF16),
         ),
         in_specs=[on_chip if name in given else far for name in INPUTS],
         out_specs=(on_chip,) * 6,
         scratch_shapes=list(scratch.values()),
         compiler_params=pltpu.CompilerParams(
-            collective_id=0, has_side_effects=True, vmem_limit_bytes=67043328
+            collective_id=0, has_side_effects=True, vmem_limit_bytes=50 << 20
         ),
     )(
-        block_input,
-        cotangent,
+        in_hbm(block_input),
+        in_hbm(cotangent),
         jnp.transpose(routes),
         jnp.transpose(route_weights),
-        gate_weight,
-        up_weight,
-        down_weight,
-        out_weight,
-        conv_out,
-        gate_pre,
-        prior_states,
-        recur_weight,
-        input_gate_matrix,
+        in_hbm(gate_weight),
+        in_hbm(up_weight),
+        in_hbm(down_weight),
+        in_hbm(out_weight),
+        in_hbm(conv_out),
+        in_hbm(gate_pre),
+        in_hbm(prior_states),
+        in_hbm(recur_weight),
+        in_hbm(input_gate_matrix),
         decay_param.reshape(columns, channels),
-        decay_jump,
+        in_hbm(decay_jump),
     )
+    return pl.pallas_call(
+        export_kernel,
+        out_shape=[jax.ShapeDtypeStruct(x.shape, x.dtype) for x in results],
+        in_specs=[on_chip] * len(results),
+        out_specs=[far] * len(results),
+        scratch_shapes=[pltpu.SemaphoreType.DMA((len(results),))],
+        compiler_params=pltpu.CompilerParams(vmem_limit_bytes=1 << 20),
+    )(*results)
 
 
 def solution(mesh):

time: 107 us -> 93.1 us (0.87)
  local copies, waits for them, and re-layouts: 11.5 us -> 0 us
  Pallas kernels: 94.2 us -> 92.1 us
    unnamed x16 -> x0, local copies, waits for them, and re-layouts: 11.5 us -> none
    pallas_call x1, Pallas kernels: 94.2 us -> 87.8 us  [local(): pl.pallas_call(functools.partial(kernel, INPUTS + OUTPUTS + tuple(scratch...]
    pallas_call x0 -> x1, Pallas kernels: none -> 4.31 us  [local(): pl.pallas_call(export_kernel, out_shape=[jax.ShapeDtypeStruct(x.shape, x....]
where the time goes in v2:
time: 93.1 us; the launch traced here: 92.9 us
  Pallas kernels  92.1 us (99%)
    pallas_call x1, Pallas kernels, local(): pl.pallas_call(functools.partial(kernel, INPUTS + OUTPUTS + tuple(scratch...  87.8 us
    pallas_call x1, Pallas kernels, local(): pl.pallas_call(export_kernel, out_shape=[jax.ShapeDtypeStruct(x.shape, x....  4.31 us

profile of v2, /device:TPU:0, one launch (start us, length us, event | category | flops | bytes accessed | tf_op | source)
XLA Modules:
  0.0 92.9 jit_solution(15121543873596444622)
XLA Ops:
  0.6 87.8 %shard_map.190 = (bf16[1,2048,896]{2,1,0:T(8,128)(2,1)S(1)}, bf16[1,2048,896]{2,1,0:T(8,128)(2,1)S(1)}, bf16[1,896,2048]{2,1,0:T(8,128)(2,1)S(1)}, f32[128,512]{...) custom-call(bf16[256,256]{1,0:T(8,128)(2,1)} %refs_0_.1, bf16[256,256]{1,0:T(8,128)(2,1)} %refs_1_.1, ...), custom_call_target="tpu_custom_call" | custom-call | tf_op jit(solution)/shard_map/pallas_call | solution.py:677
  88.4 4.3 %shard_map.191 = (bf16[1,2048,896]{2,1,0:T(8,128)(2,1)}, bf16[1,2048,896]{2,1,0:T(8,128)(2,1)}, bf16[1,896,2048]{2,1,0:T(8,128)(2,1)}, f32[128,512]{1,0:T(8,128)...) custom-call(bf16[1,2048,896]{2,1,0:T(8,128)(2,1)S(1)} %get-tuple-element.12.refs_0_, ...), custom_call_target="tpu_custom_call" | custom-call | tf_op jit(solution)/shard_map/pallas_call | solution.py:710

commit v3 on v2

--- a/solution.py
+++ b/solution.py
@@ -81,17 +81,18 @@
         else:
             pl.when(when)(action)
 
-    def finish(self):
-        for when, copy in self.sent:
+    def finish(self, amount=None):
+        amount = len(self.sent) if amount is None else amount
+        for when, copy in self.sent[:amount]:
             self.run(when, copy.wait_send)
-        self.sent = []
+        self.sent = self.sent[amount:]
 
 
 INPUTS = (
     "rows_hbm", "cot_hbm", "routes", "route_w", "wg_hbm", "wu_hbm", "wd_hbm", "ow_hbm",
     "conv_hbm", "pre_hbm", "prior_hbm", "wr_hbm", "wi_hbm", "rate", "jump_hbm",
 )
-OUTPUTS = ("gate_grad", "up_grad", "down_grad", "out_grad", "conv_grad", "valve")
+OUTPUTS = ("gate_grad", "down_grad", "out_grad", "conv_grad", "valve", "slot_rows", "d_up")
 
 
 class Refs:
@@ -199,9 +200,10 @@
                 plane[a, d, k].wait_recv()
         here = filled[a].at[:, here_of(d)]
         forward[a, d] = copies.start(here, here, partner)[1]
-        if d == 0 and a == relieved[0]:
-            there = r.slot_cot.at[:, here_of(0)]
-            line[relieved] = copies.start(there, there, lines[relieved[1]])[1]
+
+    def relieve():
+        there = filled[relieved[0]].at[:, here_of(0)]
+        line[relieved] = copies.start(there, there, lines[relieved[1]])[1]
 
     def row_loop(body):
         size = total // 2
@@ -335,6 +337,8 @@
             scoped("between", between[i])
         if i + 2 < count:
             scoped(f"issue#i={i + 2}", issue, *stages[i + 2])
+        if i + 2 == count - 1 - (deep - 1 > 2):
+            relieve()
         if i == count - 1:
             scoped("pass_on_relieved", pass_on, *relieved)
             scoped("absorb_relieved", absorb, *stages[i - 1])
@@ -365,17 +369,12 @@
         rows = r.slot_rows[:, span(i, wide)]
         r.gate_grad[0, span(i, wide), :] = dot(rows, r.d_gate[...], TN).astype(BF16)
 
-    def up_block(i):
-        rows = r.slot_rows[:, span(i, wide)]
-        r.up_grad[0, span(i, wide), :] = dot(rows, r.d_up[...], TN).astype(BF16)
-
     def down_block(i):
         cols = span(i, wide)
         r.down_grad[0, :, cols] = dot(r.hidden[...], r.slot_cot[:, cols], TN).astype(BF16)
 
     blocks_of(down_block, full // wide, 2)
     blocks_of(gate_block, full // wide, 2)
-    blocks_of(up_block, full // wide, 2)
 
     def fill(amount):
         for _ in range(amount):
@@ -467,14 +466,22 @@
         return r.piece_sems.at[(slot * share + q) * halves + h]
 
     def use(d, h):
+        mix(d, h)
+        spread(d, h)
+
+    def mix(d, h):
         shared[d, h].wait_recv()
+        value = None if d == 0 and h == 0 else r.d_mixed[...]
+        for c in range(CORES):
+            cols = span((levels[d] * CORES + c) * halves + h, half)
+            part = dot(r.ow[:, cols], r.block_grad[:, cols], NT)
+            value = part if value is None else value + part
+        r.d_mixed[...] = value
+
+    def spread(d, h):
         for c in range(CORES):
             block = levels[d] * CORES + c
-            cols = span(block * halves + h, half)
-            grads = r.block_grad[:, cols]
-            value = dot(r.ow[:, cols], grads, NT)
-            start = d == 0 and h == 0 and c == 0
-            r.d_mixed[...] = value if start else r.d_mixed[...] + value
+            grads = r.block_grad[:, span(block * halves + h, half)]
             r.product[d, h, c] = dot(r.mixed[...], grads).astype(BF16)
             to, q = lax.div(block, share), lax.rem(block, share)
             copy = pltpu.make_async_remote_copy(
@@ -509,8 +516,10 @@
             if h and i == 0:
                 scoped("sum", close_sum, h - 1)
             if h and i == 2:
+                fill(1)
                 scoped("gather", gather, 1, h - 1)
             if h and i == 3:
+                fill(1)
                 scoped("gather", gather, 2, h - 1)
                 for e in range(3, deep):
                     scoped("gather", gather, e, h - 1)
@@ -525,8 +534,10 @@
     for d in range(1, deep):
         scoped("gather", gather, d, halves - 1)
         if d > 1:
-            scoped("use", use, d - 1, halves - 1)
-    scoped("use", use, deep - 1, halves - 1)
+            scoped("mix", mix, d - 1, halves - 1)
+        if d == 2:
+            scoped("spread", spread, 1, halves - 1)
+    scoped("mix", mix, deep - 1, halves - 1)
 
     d_mixed = r.d_mixed[...]
     value = d_mixed * r.keep[4]
@@ -543,6 +554,10 @@
         tails.append(copies.start(r.summary, r.summaries.at[sp], planes[k])[1])
     r.summaries[sp] = r.summary[...]
     r.valve[...] = (d_mixed * r.keep[3]).astype(BF16)
+    for d in range(2, deep):
+        scoped("spread", spread, d, halves - 1)
+    with jax.named_scope("settle"):
+        copies.finish(len(copies.sent) - (deep - 2) * CORES - experts)
     with jax.named_scope("summaries"):
         for copy in tails:
             copy.wait_recv()
@@ -578,14 +593,25 @@
     copies.finish()
 
 
-def export_kernel(*refs):
-    count = (len(refs) - 1) // 2
-    copies = [
-        pltpu.make_async_copy(refs[i], refs[count + i], refs[-1].at[i]) for i in range(count)
+def export_kernel(gate, down, out, conv, valve, rows, d_up, *refs):
+    outs, (block, sems, up_sems) = refs[:6], refs[6:]
+    whole = [
+        pltpu.make_async_copy(a, b, sems.at[i])
+        for i, (a, b) in enumerate(zip((gate, down, out, conv, valve), outs))
     ]
-    for copy in copies:
+    for copy in whole:
         copy.start()
-    for copy in copies:
+    wide = block.shape[1]
+    steps = rows.shape[1] // wide
+    pieces = []
+    for i in range(steps):
+        part = pl.ds(i * wide, wide)
+        block[i] = dot(rows[:, part], d_up[...], TN).astype(BF16)
+        pieces.append(
+            pltpu.make_async_copy(block.at[i], outs[5].at[0, part, :], up_sems.at[i])
+        )
+        pieces[-1].start()
+    for copy in whole + pieces:
         copy.wait()
 
 
@@ -639,14 +665,12 @@
         taking=vmem((tokens, total), BF16),
         slot_weight=vmem((total, 1), F32),
         stage=vmem((2, deep, total, width), BF16),
-        slot_rows=vmem((total, full), BF16),
         slot_cot=vmem((total, full), BF16),
         acc_gate=vmem((total, units), F32),
         acc_up=vmem((total, units), F32),
         acc_hidden=vmem((total, units), F32),
         hidden=vmem((total, units), BF16),
         d_gate=vmem((total, units), BF16),
-        d_up=vmem((total, units), BF16),
         paired=vmem((deep, total, width), BF16),
         homed=vmem((halves, deep, total, half), BF16),
         line_out=vmem((halves, deep - 1, tokens, half), BF16),
@@ -678,14 +702,15 @@
         functools.partial(kernel, INPUTS + OUTPUTS + tuple(scratch), experts, deep, cap),
         out_shape=(
             vmem(gate_weight.shape, BF16),
-            vmem(up_weight.shape, BF16),
             vmem(down_weight.shape, BF16),
             vmem((channels, full // experts), F32),
             vmem((channels, length), BF16),
             vmem((channels, length), BF16),
+            vmem((total, full), BF16),
+            vmem((total, units), BF16),
         ),
         in_specs=[on_chip if name in given else far for name in INPUTS],
-        out_specs=(on_chip,) * 6,
+        out_specs=(on_chip,) * len(OUTPUTS),
         scratch_shapes=list(scratch.values()),
         compiler_params=pltpu.CompilerParams(
             collective_id=0, has_side_effects=True, vmem_limit_bytes=50 << 20
@@ -707,14 +732,21 @@
         decay_param.reshape(columns, channels),
         in_hbm(decay_jump),
     )
-    return pl.pallas_call(
+    wide = 256
+    saved = [jax.ShapeDtypeStruct(x.shape, x.dtype) for x in results[:5]]
+    gate, down, out, conv, valve, up = pl.pallas_call(
         export_kernel,
-        out_shape=[jax.ShapeDtypeStruct(x.shape, x.dtype) for x in results],
+        out_shape=saved + [jax.ShapeDtypeStruct(up_weight.shape, BF16)],
         in_specs=[on_chip] * len(results),
-        out_specs=[far] * len(results),
-        scratch_shapes=[pltpu.SemaphoreType.DMA((len(results),))],
-        compiler_params=pltpu.CompilerParams(vmem_limit_bytes=1 << 20),
+        out_specs=[far] * 6,
+        scratch_shapes=[
+            vmem((full // wide, wide, units), BF16),
+            pltpu.SemaphoreType.DMA((5,)),
+            pltpu.SemaphoreType.DMA((full // wide,)),
+        ],
+        compiler_params=pltpu.CompilerParams(vmem_limit_bytes=12 << 20),
     )(*results)
+    return gate, up, down, out, conv, valve
 
 
 def solution(mesh):

time: 93.1 us -> 87.6 us (0.941)
  Pallas kernels: 92.1 us -> 86.6 us
    pallas_call x1, Pallas kernels: 87.8 us -> 80.7 us  [local(): pl.pallas_call(functools.partial(kernel, INPUTS + OUTPUTS + tuple(scratch...]
    pallas_call x1, Pallas kernels: 4.31 us -> 5.91 us  [local(): pl.pallas_call(export_kernel, out_shape=saved + [jax.ShapeDtypeStruct(up_...]
where the time goes in v3:
time: 87.6 us; the launch traced here: 87.4 us
  Pallas kernels  86.6 us (99%)
    pallas_call x1, Pallas kernels, local(): pl.pallas_call(functools.partial(kernel, INPUTS + OUTPUTS + tuple(scratch...  80.7 us
    pallas_call x1, Pallas kernels, local(): pl.pallas_call(export_kernel, out_shape=saved + [jax.ShapeDtypeStruct(up_...  5.91 us

profile of v3, /device:TPU:0, one launch (start us, length us, event | category | flops | bytes accessed | tf_op | source)
XLA Modules:
  0.0 87.4 jit_solution(9659881325806991969)
XLA Ops:
  0.6 80.7 %shard_map.190 = (bf16[1,2048,896]{2,1,0:T(8,128)(2,1)S(1)}, bf16[1,896,2048]{2,1,0:T(8,128)(2,1)S(1)}, f32[128,512]{1,0:T(8,128)S(1)}, bf16[128,256]{1,0:T(8,12...) custom-call(bf16[256,256]{1,0:T(8,128)(2,1)} %refs_0_.1, ...), custom_call_target="tpu_custom_call" | custom-call | tf_op jit(solution)/shard_map/pallas_call | solution.py:701
  81.3 5.9 %shard_map.191 = (bf16[1,2048,896]{2,1,0:T(8,128)(2,1)}, bf16[1,896,2048]{2,1,0:T(8,128)(2,1)}, f32[128,512]{1,0:T(8,128)}, bf16[128,256]{1,0:T(8,128)(2,1)}, bf...) custom-call(bf16[1,2048,896]{2,1,0:T(8,128)(2,1)S(1)} %get-tuple-element.19.gate, ...), custom_call_target="tpu_custom_call" | custom-call | tf_op jit(solution)/shard_map/pallas_call | solution.py:737

commit v4 on v3

--- a/solution.py
+++ b/solution.py
@@ -58,22 +58,44 @@
 class Copies:
     def __init__(self, send_sems, recv_sems):
         self.sems = (send_sems, recv_sems)
-        self.count = 0
+        self.sends, self.arrivals, self.count = 0, 0, 0
         self.sent = []
 
-    def start(self, source, target, device, when=None, arrival=None):
-        index, self.count = self.count, self.count + 1
-        copy = pltpu.make_async_remote_copy(
+    def make(self, source, target, device, send, arrival):
+        return pltpu.make_async_remote_copy(
             src_ref=source,
             dst_ref=target,
-            send_sem=self.sems[0].at[index],
-            recv_sem=self.sems[1].at[index if arrival is None else arrival],
+            send_sem=self.sems[0].at[send],
+            recv_sem=self.sems[1].at[arrival],
             device_id=device,
             device_id_type=pl.DeviceIdType.MESH,
         )
+
+    def take_send(self):
+        send, self.sends = self.sends, self.sends + 1
+        self.count = max(self.count, self.sends)
+        assert self.sends <= self.sems[0].shape[0]
+        return send
+
+    def take_arrival(self):
+        arrival, self.arrivals = self.arrivals, self.arrivals + 1
+        assert self.arrivals <= self.sems[1].shape[0]
+        return arrival
+
+    def start(self, source, target, device, when=None, arrival=None):
+        arrival = self.take_arrival() if arrival is None else arrival
+        copy = self.make(source, target, device, self.take_send(), arrival)
         self.run(when, copy.start)
         self.sent.append((when, copy))
-        return index, copy
+        return arrival, copy
+
+    def start_all(self, pairs, sent, landed, device):
+        send, arrival = self.take_send(), self.take_arrival()
+        for source, target, to in pairs:
+            self.make(source, target, to, send, arrival).start()
+        copy = self.make(sent, landed, device, send, arrival)
+        self.sent.append((None, copy))
+        return copy
 
     def run(self, when, action):
         if when is None:
@@ -86,6 +108,8 @@
         for when, copy in self.sent[:amount]:
             self.run(when, copy.wait_send)
         self.sent = self.sent[amount:]
+        if not self.sent:
+            self.sends = 0
 
 
 INPUTS = (
@@ -184,20 +208,27 @@
         if a:
             placed = placed * r.slot_weight[...]
         r.stage[a, d] = placed.astype(BF16)
-        for k in range(1, experts):
-            plane[a, d, k] = copies.start(
-                r.stage.at[a, d, span(planes[k][0], cap)],
-                filled[a].at[span(sp, cap), here_of(d)],
-                planes[k],
-            )[1]
+        others = pl.ds(0, (experts - 1) * cap)
+        plane[a, d] = copies.start_all(
+            [
+                (
+                    r.stage.at[a, d, span(planes[k][0], cap)],
+                    filled[a].at[span(sp, cap), here_of(d)],
+                    planes[k],
+                )
+                for k in range(1, experts)
+            ],
+            r.stage.at[a, d, others],
+            filled[a].at[others, here_of(d)],
+            planes[1],
+        )
         filled[a][span(sp, cap), here_of(d)] = r.stage[a, d, span(sp, cap), :]
 
     def pass_on(a, d):
         if (a, d) == relieved:
             line[a, d].wait_recv()
         else:
-            for k in range(1, experts):
-                plane[a, d, k].wait_recv()
+            plane[a, d].wait_recv()
         here = filled[a].at[:, here_of(d)]
         forward[a, d] = copies.start(here, here, partner)[1]
 
@@ -391,20 +422,21 @@
         first = d % room * width + start
         return (r.acc_gate, r.acc_up, r.acc_hidden)[d // room], slice(first, first + size)
 
-    def pair_block(d):
+    def width_block(d, which):
         def chunk(rows):
             gate, up = r.d_gate[rows, :], r.d_up[rows, :]
-            for which, block in enumerate((levels[d] * CORES + 1 - core, levels[d] * CORES + core)):
-                value = dot(gate, r.wg[span(block, width), :], NT)
-                value = value + dot(up, r.wu[span(block, width), :], NT)
-                if which:
+            for side in which:
+                block = span(levels[d] * CORES + (core if side else 1 - core), width)
+                value = dot(gate, r.wg[block, :], NT) + dot(up, r.wu[block, :], NT)
+                if side:
                     kept, cols = kept_of(d, 0, width)
                     kept[rows, cols] = value
                 else:
                     r.stage[0, d, rows, :] = value.astype(BF16)
 
         row_loop(chunk)
-        core_copy[d] = copies.start(r.stage.at[0, d], r.paired.at[d], partner)[1]
+        if 0 in which:
+            core_copy[d] = copies.start(r.stage.at[0, d], r.paired.at[d], partner)[1]
 
     def ship(d, h):
         if h == 0:
@@ -413,17 +445,24 @@
         kept, kept_cols = kept_of(d, h * half, half)
         joint = kept[:, kept_cols] + r.paired[d, :, cols].astype(F32)
         r.stage[1, d, :, cols] = joint.astype(BF16)
-        for k in range(1, experts):
-            home_copy[d, h, k] = copies.start(
-                r.stage.at[1, d, span(planes[k][0], cap), pl.ds(h * half, half)],
-                r.homed.at[h, d, span(sp, cap)],
-                planes[k],
-            )[1]
+        part, others = pl.ds(h * half, half), pl.ds(0, (experts - 1) * cap)
+        home_copy[d, h] = copies.start_all(
+            [
+                (
+                    r.stage.at[1, d, span(planes[k][0], cap), part],
+                    r.homed.at[h, d, span(sp, cap)],
+                    planes[k],
+                )
+                for k in range(1, experts)
+            ],
+            r.stage.at[1, d, others, part],
+            r.homed.at[h, d, others],
+            planes[1],
+        )
         r.homed[h, d, span(sp, cap), :] = r.stage[1, d, span(sp, cap), cols]
 
     def home(d, h):
-        for k in range(1, experts):
-            home_copy[d, h, k].wait_recv()
+        home_copy[d, h].wait_recv()
         summed = dot(r.taking[...], r.homed[h, d])
         if d:
             r.line_out[h, d - 1] = summed.astype(BF16)
@@ -462,8 +501,8 @@
     share = (full // experts) // width
     pieces = {}
 
-    def arrival_of(slot, q, h):
-        return r.piece_sems.at[(slot * share + q) * halves + h]
+    def arrival_of(slot):
+        return r.piece_sems.at[slot]
 
     def use(d, h):
         mix(d, h)
@@ -488,7 +527,7 @@
                 src_ref=r.product.at[d, h, c],
                 dst_ref=r.products.at[sp, q, h],
                 send_sem=r.sent_sems.at[(d * halves + h) * CORES + c],
-                recv_sem=arrival_of(sp, q, h),
+                recv_sem=arrival_of(sp),
                 device_id=(to, tp),
                 device_id_type=pl.DeviceIdType.MESH,
             )
@@ -501,43 +540,61 @@
 
     with jax.named_scope("settle"):
         copies.finish()
-    scoped("pair", pair_block, order[0])
-    for i, d in enumerate(order):
-        if i + 1 < deep:
-            scoped("pair", pair_block, order[i + 1])
-        scoped("ship", ship, d, 0)
+    waiting = [(order[0], h) for h in range(halves)]
+    waiting += [(d, h) for h in range(halves) for d in order[1:]]
+
+    def next_home():
+        d, h = waiting.pop(0)
+        scoped(f"home#h={h}#d={d}", home, d, h)
+        return d, h
+
+    scoped("theirs", width_block, order[0], (0,))
+    scoped("mine", width_block, order[0], (1,))
+    for h in range(halves):
+        scoped("ship", ship, order[0], h)
+    scoped("pair", width_block, order[1], (0, 1))
+    for i in range(2, deep + 1):
+        if i < deep:
+            scoped("pair", width_block, order[i], (0, 1))
+        scoped("ship", ship, order[i - 1], 0)
+        if i < deep:
+            next_home()
+        if i == deep - 1:
+            fill(1)
     for h in range(1, halves):
-        for d in order:
+        for d in order[1:]:
             scoped("ship", ship, d, h)
-    for h in range(halves):
-        for i, d in enumerate(order):
+    while waiting:
+        d, h = next_home()
+        if h and d == order[1]:
+            scoped("sum", close_sum, h - 1)
+        if h and d == order[-1]:
+            for e in range(1, 3):
+                scoped("gather", gather, e, h - 1)
+        if (d, h) != (order[-1], halves - 1):
             fill(1)
-            scoped(f"home#h={h}#d={d}", home, d, h)
-            if h and i == 0:
-                scoped("sum", close_sum, h - 1)
-            if h and i == 2:
-                fill(1)
-                scoped("gather", gather, 1, h - 1)
-            if h and i == 3:
-                fill(1)
-                scoped("gather", gather, 2, h - 1)
-                for e in range(3, deep):
-                    scoped("gather", gather, e, h - 1)
-                for e in range(2):
-                    scoped("use", use, e, h - 1)
-    scoped("sum", close_sum, halves - 1)
-    for h in range(halves - 1):
-        for d in range(2, deep):
+    last = halves - 1
+    scoped("sum", close_sum, last)
+    for h in range(last):
+        for d in range(2):
             scoped("use", use, d, h)
+        for d in range(3, deep):
+            scoped("gather", gather, d, h)
+        scoped("use", use, 2, h)
+    fill(1)
+    scoped("gather", gather, 1, last)
+    for h in range(last):
+        for d in range(3, deep):
+            scoped("use", use, d, h)
+    scoped("use", use, 0, last)
+    scoped("gather", gather, 2, last)
     fill(100)
-    scoped("use", use, 0, halves - 1)
-    for d in range(1, deep):
-        scoped("gather", gather, d, halves - 1)
-        if d > 1:
-            scoped("mix", mix, d - 1, halves - 1)
-        if d == 2:
-            scoped("spread", spread, 1, halves - 1)
-    scoped("mix", mix, deep - 1, halves - 1)
+    scoped("mix", mix, 1, last)
+    scoped("spread", spread, 1, last)
+    for d in range(3, deep):
+        scoped("gather", gather, d, last)
+        scoped("mix", mix, d - 1, last)
+    scoped("mix", mix, deep - 1, last)
 
     d_mixed = r.d_mixed[...]
     value = d_mixed * r.keep[4]
@@ -547,20 +604,22 @@
         reach *= 2
         level += 1
     decay_first = r.keep[5][:, 0:1]
-    r.summary[0:1, :] = to_row(decay_first * r.keep[6][:, 0:1])
-    r.summary[1:2, :] = to_row(decay_first * value[:, 0:1])
-    tails = []
-    for k in range(1, experts):
-        tails.append(copies.start(r.summary, r.summaries.at[sp], planes[k])[1])
-    r.summaries[sp] = r.summary[...]
+    r.summary[0, 0:1, :] = to_row(decay_first * r.keep[6][:, 0:1])
+    r.summary[0, 1:2, :] = to_row(decay_first * value[:, 0:1])
+    ends = copies.start_all(
+        [(r.summary.at[0], r.summaries.at[sp], planes[k]) for k in range(1, experts)],
+        r.summary.at[pl.ds(0, experts - 1)],
+        r.summaries.at[pl.ds(0, experts - 1)],
+        planes[1],
+    )
+    r.summaries[sp] = r.summary[0]
     r.valve[...] = (d_mixed * r.keep[3]).astype(BF16)
     for d in range(2, deep):
         scoped("spread", spread, d, halves - 1)
     with jax.named_scope("settle"):
-        copies.finish(len(copies.sent) - (deep - 2) * CORES - experts)
+        copies.finish(len(copies.sent) - (deep - 2) * CORES - 1)
     with jax.named_scope("summaries"):
-        for copy in tails:
-            copy.wait_recv()
+        ends.wait_recv()
     carried = jnp.zeros((1, channels), F32)
     for later in range(experts - 1, 0, -1):
         longer = r.summaries[later, 1:2, :] + r.summaries[later, 0:1, :] * carried
@@ -573,24 +632,24 @@
     r.conv_grad[...] = conv_grad.astype(BF16)
     with jax.named_scope("products"):
         for k in range(1, experts):
-            for q in range(share):
-                for h in range(halves):
-                    spot = r.products.at[planes[k][0], q, h]
-                    pltpu.make_async_remote_copy(
-                        src_ref=r.product.at[0, 0, 0],
-                        dst_ref=spot,
-                        send_sem=r.sent_sems.at[0],
-                        recv_sem=arrival_of(planes[k][0], q, h),
-                        device_id=planes[k],
-                        device_id_type=pl.DeviceIdType.MESH,
-                    ).wait_recv()
-    for q in range(share):
-        for h in range(halves):
-            value = r.products[0, q, h].astype(F32)
-            for e in range(1, experts):
-                value = value + r.products[e, q, h].astype(F32)
-            r.out_grad[:, q * width + h * half : q * width + (h + 1) * half] = value
-    copies.finish()
+            spot = r.products.at[planes[k][0]]
+            pltpu.make_async_remote_copy(
+                src_ref=spot,
+                dst_ref=spot,
+                send_sem=r.sent_sems.at[0],
+                recv_sem=arrival_of(planes[k][0]),
+                device_id=planes[k],
+                device_id_type=pl.DeviceIdType.MESH,
+            ).wait_recv()
+    with jax.named_scope("assemble"):
+        for q in range(share):
+            for h in range(halves):
+                value = r.products[0, q, h].astype(F32)
+                for e in range(1, experts):
+                    value = value + r.products[e, q, h].astype(F32)
+                r.out_grad[:, q * width + h * half : q * width + (h + 1) * half] = value
+    with jax.named_scope("finish"):
+        copies.finish()
 
 
 def export_kernel(gate, down, out, conv, valve, rows, d_up, *refs):
@@ -645,7 +704,10 @@
     halves = max(1, width // 128)
     half = width // halves
     share = (full // experts) // width
-    copies = 2 * deep * (experts + 2) + deep + halves * deep * (experts + 4) + experts
+    relays = int(deep == 4)
+    in_dispatch = 3 * (2 * deep - 1) + 2 * relays
+    in_combine = deep + halves * (4 * deep - 2) + 1
+    sends = max(in_dispatch, in_combine + halves * relays)
     vmem = pltpu.VMEM
     scratch = dict(
         rows=vmem((tokens, width), BF16),
@@ -683,13 +745,13 @@
         reach=vmem((doublings, channels, length), F32),
         product=vmem((deep, halves, CORES, channels, half), BF16),
         products=vmem((experts, share, halves, channels, half), BF16),
-        summary=vmem((8, channels), F32),
+        summary=vmem((experts - 1, 8, channels), F32),
         summaries=vmem((experts, 8, channels), F32),
-        send_sems=pltpu.SemaphoreType.DMA((copies,)),
-        recv_sems=pltpu.SemaphoreType.DMA((copies,)),
+        send_sems=pltpu.SemaphoreType.DMA((sends,)),
+        recv_sems=pltpu.SemaphoreType.DMA((in_dispatch + in_combine,)),
         local_sems=pltpu.SemaphoreType.DMA((12,)),
         sent_sems=pltpu.SemaphoreType.DMA((deep * halves * CORES,)),
-        piece_sems=pltpu.SemaphoreType.DMA((experts * share * halves,)),
+        piece_sems=pltpu.SemaphoreType.DMA((experts,)),
     )
     on_chip = pl.BlockSpec(memory_space=pltpu.VMEM)
     far = pl.BlockSpec(memory_space=pltpu.HBM)

time: 87.6 us -> 81.4 us (0.929)
  Pallas kernels: 86.6 us -> 80.4 us
    pallas_call x1, Pallas kernels: 80.7 us -> 74.5 us  [local(): pl.pallas_call(functools.partial(kernel, INPUTS + OUTPUTS + tuple(scratch...]
where the time goes in v4:
time: 81.4 us; the launch traced here: 81.2 us
  Pallas kernels  80.4 us (99%)
    pallas_call x1, Pallas kernels, local(): pl.pallas_call(functools.partial(kernel, INPUTS + OUTPUTS + tuple(scratch...  74.5 us
    pallas_call x1, Pallas kernels, local(): pl.pallas_call(export_kernel, out_shape=saved + [jax.ShapeDtypeStruct(up_...  5.91 us

profile of v4, /device:TPU:0, one launch (start us, length us, event | category | flops | bytes accessed | tf_op | source)
XLA Modules:
  0.0 81.2 jit_solution(3292747544963777564)
XLA Ops:
  0.6 74.5 %shard_map.190 = (bf16[1,2048,896]{2,1,0:T(8,128)(2,1)S(1)}, bf16[1,896,2048]{2,1,0:T(8,128)(2,1)S(1)}, f32[128,512]{1,0:T(8,128)S(1)}, bf16[128,256]{1,0:T(8,12...) custom-call(bf16[256,256]{1,0:T(8,128)(2,1)} %refs_0_.1, ...), custom_call_target="tpu_custom_call" | custom-call | tf_op jit(solution)/shard_map/pallas_call | solution.py:763
  75.1 5.9 %shard_map.191 = (bf16[1,2048,896]{2,1,0:T(8,128)(2,1)}, bf16[1,896,2048]{2,1,0:T(8,128)(2,1)}, f32[128,512]{1,0:T(8,128)}, bf16[128,256]{1,0:T(8,128)(2,1)}, bf...) custom-call(bf16[1,2048,896]{2,1,0:T(8,128)(2,1)S(1)} %get-tuple-element.19.gate, ...), custom_call_target="tpu_custom_call" | custom-call | tf_op jit(solution)/shard_map/pallas_call | solution.py:799
